TPU v7x, 512 devices: a whole 4x4x16 slice. The times are simulated.
512 devices in a mesh: sp: 32 (over z, core), tp: 16 (over y, x).
Axes of the slice: x: 4, y: 4, z: 16, core: 2. Of those that a mesh axis runs over, the one named last changes fastest.
Arguments:
- residual_signal: bfloat16 [4096, 2048], P(('sp', 'tp')), may hold values from -6 to 6
- prelayer_scaling_factor: float32 [2048], replicated, may hold values from 0.1 to 1.9
- result_adjoint: bfloat16 [4096, 2048], P(('sp', 'tp')), may hold values from -24 to 24
- chosen_specialist_ids: int32 [4096, 2], P('sp'), may hold values from 0 to 31, all different within a row; in each aligned block of 128 rows (0 to 127, 128 to 255, ...) at most 10 rows name the same one
- dispatch_shares: float32 [4096, 2], P('sp'), may hold values from 0.2 to 1
- specialist_valve_matrix: bfloat16 [32, 2048, 2048], P('sp', None, 'tp'), may hold values from -0.125 to 0.125
- specialist_widen_matrix: bfloat16 [32, 2048, 2048], P('sp', None, 'tp'), may hold values from -0.125 to 0.125
- specialist_shrink_matrix: bfloat16 [32, 2048, 2048], P('sp', 'tp'), may hold values from -0.125 to 0.125
- probe_vectors: bfloat16 [4096, 1024], P('sp'), may hold values from -6 to 6
- lookup_vectors: bfloat16 [4096, 1024], P('sp'), may hold values from -1.5 to 1.5
- persistence_scores: bfloat16 [4096, 1024], P('sp'), may hold values from -2 to 8
- group_additional_shrinkage: float32 [4096, 2], P('sp'), may hold values from -4.2 to 0
- content_vectors: bfloat16 [4096, 2, 1024], P('sp', None, 'tp'), may hold values from -6 to 6
- result_valve_scores: bfloat16 [4096, 2, 1024], P('sp', None, 'tp'), may hold values from -6 to 6
- stored_opening_memory: float32 [32, 2, 512, 1024], P('sp', None, None, 'tp'), may hold values from -24 to 24
- result_mapping_matrix: bfloat16 [2048, 2, 1024], P(None, None, 'tp'), may hold values from -0.125 to 0.125
Outputs:
- stream_grad: bfloat16 [4096, 2048], P(('sp', 'tp'))
- gate_grad: bfloat16 [32, 2048, 2048], P('sp', None, 'tp')
- up_grad: bfloat16 [32, 2048, 2048], P('sp', None, 'tp')
- down_grad: bfloat16 [32, 2048, 2048], P('sp', 'tp')
- proj_grad: float32 [2048, 2, 1024], P('sp', None, 'tp')
- query_grad: bfloat16 [4096, 1024], P('sp', 'tp')
- key_grad: bfloat16 [4096, 1024], P('sp', 'tp')
- retain_preact_derivative: float32 [4096, 1024], P('sp', 'tp')
- value_grad: bfloat16 [4096, 2, 1024], P('sp', None, 'tp')
- gate_input_grad: bfloat16 [4096, 2, 1024], P('sp', None, 'tp')
Inputs may be any that keep to these rules, and one draw needn't show every extreme that they name: `chosen_specialist_ids`: the 2 experts of a token differ. In each aligned block of 128 tokens no expert is named by more than 10 tokens, a bound that some expert reaches in some block.
All inputs are finite; a program needn't handle non-finite values.
Results may differ from a plain program's by a relative error of at most 0.028.
Values may be sent and summed in bfloat16 or wider, within the bound.
A program may use at most 64 MiB of HBM per device.

v0:
```python
import jax
import jax.numpy as jnp
from jax import lax
from jax.sharding import Mesh
from jax.sharding import PartitionSpec as P

PIECE_PLACES = 64
SP = ("sp_0", "sp_1")
SP_TP = ("sp_0", "sp_1", "tp")


toggle_smoothness = 16.0
norm_eps = 1e-06


def from_everyone(shard, axis):
    copies = jnp.broadcast_to(shard, (lax.axis_size(axis), *shard.shape))
    return lax.all_to_all(copies, axis, split_axis=0, concat_axis=0, tiled=True)


def joined_along(tiles, dim):
    tiles = jnp.moveaxis(tiles, 0, dim)
    shape = tiles.shape
    return tiles.reshape(*shape[:dim], shape[dim] * shape[dim + 1], *shape[dim + 2 :])


def gather_directly(shard, axis, dim):
    tiles = from_everyone(shard, axis)
    return joined_along(tiles, dim)


def cut_along(shard, dim, length):
    shape = shard.shape
    tiles = shard.reshape(*shape[:dim], length, shape[dim] // length, *shape[dim + 1 :])
    return jnp.moveaxis(tiles, dim, 0)


def sum_at_owner(shard, axis, dim):
    length = lax.axis_size(axis)
    tiles = lax.all_to_all(cut_along(shard, dim, length), axis, 0, 0, tiled=True)
    return jnp.sum(tiles.astype(jnp.float32), axis=0)


def filled_with(shard, identity):
    return jax.tree.map(
        lambda a, e: jnp.broadcast_to(jnp.asarray(e, a.dtype), a.shape), shard, identity
    )


def carried_in(shard, axes, combine, identity):
    before = start = filled_with(shard, identity)
    total = shard
    for axis in reversed(axes):
        length, index = (lax.axis_size(axis), lax.axis_index(axis))
        pieces = jax.tree.map(
            lambda part, kind: lax.all_gather(part.astype(kind), axis),
            total,
            (jnp.bfloat16, jnp.bfloat16),
        )
        inside, total = (start, start)
        for k in reversed(range(length)):
            passed = k > index
            total = combine(
                total, jax.tree.map(lambda part, own: part[k].astype(own.dtype), pieces, shard)
            )
            inside = jax.tree.map(lambda new, old: jnp.where(passed, new, old), total, inside)
        before = combine(inside, before)
    return before


def sum_packed(arrays, axis, dims):
    length = lax.axis_size(axis)
    tiles = [cut_along(a, dim, length) for a, dim in zip(arrays, dims)]
    lines = jnp.concatenate([b.reshape(length, -1) for b in tiles], axis=1)
    extent = max(16, -(-lines.shape[1] // 1024) * 8)
    lines = jnp.pad(lines, ((0, 0), (0, extent * 128 - lines.shape[1]))).reshape(-1, 128)
    line, at, gathered = (lax.psum_scatter(lines, axis, tiled=True).reshape(-1), 0, [])
    for b in tiles:
        part = b[0]
        gathered.append(line[at : at + part.size].reshape(part.shape))
        at += part.size
    return tuple(gathered)


def silu_slope(value):
    sigma = jax.nn.sigmoid(value)
    return sigma + value * sigma * (1.0 - sigma)


def chain_join(first_part, second_part):
    return (
        first_part[0] * second_part[0],
        second_part[1] + second_part[0][..., None] * first_part[1],
    )


def expert_backward(routed_rows, w_gate, w_up, w_down):
    inputs = routed_rows[:, 0]
    cotangent = routed_rows[:, 1]
    contract_last = (((1,), (1,)), ((), ()))
    contract_first = (((0,), (0,)), ((), ()))
    pre_gate = jnp.dot(inputs, w_gate, preferred_element_type=jnp.float32)
    pre_up = jnp.dot(inputs, w_up, preferred_element_type=jnp.float32)
    hidden = (jax.nn.silu(pre_gate) * pre_up).astype(jnp.bfloat16)
    hidden_grad = lax.dot_general(
        cotangent, w_down, contract_last, preferred_element_type=jnp.float32
    )
    down_part = lax.dot_general(
        hidden, cotangent, contract_first, preferred_element_type=jnp.float32
    ).astype(jnp.bfloat16)
    gate_pre = (hidden_grad * pre_up * silu_slope(pre_gate)).astype(jnp.bfloat16)
    up_pre = (hidden_grad * jax.nn.silu(pre_gate)).astype(jnp.bfloat16)
    gate_part = lax.dot_general(
        inputs, gate_pre, contract_first, preferred_element_type=jnp.float32
    ).astype(jnp.bfloat16)
    up_part = lax.dot_general(
        inputs, up_pre, contract_first, preferred_element_type=jnp.float32
    ).astype(jnp.bfloat16)
    partial_value = lax.dot_general(
        gate_pre, w_gate, contract_last, preferred_element_type=jnp.float32
    ) + lax.dot_general(up_pre, w_up, contract_last, preferred_element_type=jnp.float32)
    return (partial_value.astype(jnp.bfloat16), gate_part, up_part, down_part)


def on_device(
    residual_signal,
    prelayer_scaling_factor,
    result_adjoint,
    chosen_specialist_ids,
    dispatch_shares,
    specialist_valve_matrix,
    specialist_widen_matrix,
    specialist_shrink_matrix,
    probe_vectors,
    lookup_vectors,
    persistence_scores,
    group_additional_shrinkage,
    content_vectors,
    result_valve_scores,
    stored_opening_memory,
    result_mapping_matrix,
):
    tp_count = lax.axis_size("tp")
    sp_count = lax.axis_size(SP)
    tp_index = lax.axis_index("tp")
    own_rows = residual_signal.shape[0]
    model_width = residual_signal.shape[1]
    column_width = model_width // tp_count
    paired = jnp.stack([residual_signal, result_adjoint], axis=1)
    span_pair = gather_directly(paired, "tp", 0)
    residual = span_pair[:, 0].astype(jnp.float32)
    cotangent = span_pair[:, 1]
    span_tokens = residual.shape[0]
    inv_rms = lax.rsqrt(jnp.mean(residual * residual, axis=1, keepdims=True) + norm_eps)
    unit_rows = residual * inv_rms
    moe_input = (unit_rows * prelayer_scaling_factor).astype(jnp.bfloat16)
    top_count = chosen_specialist_ids.shape[1]
    weighted = (dispatch_shares[:, :, None] * cotangent.astype(jnp.float32)[:, None, :]).astype(
        jnp.bfloat16
    )
    local_experts = specialist_valve_matrix.shape[0]
    expert_total = local_experts * sp_count
    assigned = span_tokens * top_count
    capacity = assigned // expert_total + assigned // (4 * expert_total)
    flat_ids = chosen_specialist_ids.reshape(assigned)
    one_hot = (flat_ids[:, None] == jnp.arange(expert_total, dtype=jnp.int32)[None, :]).astype(
        jnp.int32
    )
    slot_index = jnp.sum((jnp.cumsum(one_hot, axis=0) - one_hot) * one_hot, axis=1)
    destination = flat_ids * capacity + slot_index
    source_of = (
        jnp.full((expert_total * capacity,), assigned, jnp.int32)
        .at[destination]
        .set(jnp.arange(assigned, dtype=jnp.int32))
    )
    input_table = moe_input
    cot_table = weighted.reshape(assigned, model_width)
    input_table = lax.dynamic_slice_in_dim(input_table, tp_index * column_width, column_width, 1)
    cot_table = lax.dynamic_slice_in_dim(cot_table, tp_index * column_width, column_width, 1)
    send_width = input_table.shape[1]
    input_table = jnp.concatenate([input_table, jnp.zeros((1, send_width), jnp.bfloat16)], axis=0)
    cot_table = jnp.concatenate([cot_table, jnp.zeros((1, send_width), jnp.bfloat16)], axis=0)
    outgoing = jnp.stack([input_table[source_of // top_count], cot_table[source_of]], axis=1)
    outgoing = outgoing.reshape(expert_total, capacity, 2, send_width)
    arrived = lax.all_to_all(outgoing, SP, split_axis=0, concat_axis=0, tiled=True)
    arrived = gather_directly(arrived, "tp", 3)
    by_expert = jnp.moveaxis(
        arrived.reshape(sp_count, local_experts, capacity, 2, model_width), 1, 0
    )
    by_expert = by_expert.reshape(local_experts, sp_count * capacity, 2, model_width)
    partial_value, gate_grad, up_grad, down_grad = jax.vmap(expert_backward)(
        by_expert, specialist_valve_matrix, specialist_widen_matrix, specialist_shrink_matrix
    )
    partial_value = jnp.moveaxis(
        partial_value.reshape(local_experts, sp_count, capacity, model_width), 0, 1
    )
    partial_value = partial_value.reshape(sp_count * local_experts, capacity, model_width)
    summed = sum_at_owner(partial_value, "tp", 2).astype(jnp.bfloat16)
    returned = lax.all_to_all(summed, SP, split_axis=0, concat_axis=0, tiled=True)
    picked = returned.reshape(expert_total * capacity, column_width)[destination].astype(
        jnp.float32
    )
    grad_columns = jnp.sum(picked.reshape(span_tokens, top_count, column_width), axis=1)
    input_grad = gather_directly(grad_columns.astype(jnp.bfloat16), "tp", 1).astype(
        grad_columns.dtype
    )
    scaled = prelayer_scaling_factor * input_grad
    stream_full = (
        cotangent.astype(jnp.float32)
        + inv_rms * (scaled - unit_rows * jnp.mean(scaled * unit_rows, axis=1, keepdims=True))
    ).astype(jnp.bfloat16)
    stream_grad = lax.dynamic_slice_in_dim(stream_full, tp_index * own_rows, own_rows, 0)
    parallel_groups = group_additional_shrinkage.shape[1]
    key_width = probe_vectors.shape[1]
    head_key = key_width // parallel_groups
    value_part = content_vectors.shape[2]
    blocks = span_tokens // PIECE_PLACES
    query_scale = head_key ** (-0.5)

    def to_blocks(tensor):
        return tensor.reshape((blocks, PIECE_PLACES) + tensor.shape[1:])

    exponent_shrinkage = (
        jax.nn.log_sigmoid(persistence_scores.astype(jnp.float32)).reshape(
            span_tokens, parallel_groups, head_key
        )
        / toggle_smoothness
        + group_additional_shrinkage[:, :, None]
    )
    cumulative = jnp.cumsum(to_blocks(exponent_shrinkage), axis=1)
    totals = cumulative[:, -1]
    factor = jnp.exp(totals[:, None] - cumulative)
    key_weight = (
        to_blocks(lookup_vectors.reshape(span_tokens, parallel_groups, head_key)).astype(
            jnp.float32
        )
        * factor
    )
    decayed = key_weight.astype(jnp.bfloat16)
    value_blocks = to_blocks(content_vectors)
    block_terms = jnp.einsum(
        "bchk,bchv->bhkv", decayed, value_blocks, preferred_element_type=jnp.float32
    )
    running_state = stored_opening_memory[0]
    prior_list = []
    state_list = []
    for block_index in range(blocks):
        prior_list.append(running_state)
        running_state = (
            running_state * jnp.exp(totals[block_index])[:, :, None] + block_terms[block_index]
        )
        state_list.append(running_state)
    priors = jnp.stack(prior_list)
    states = jnp.stack(state_list)
    scaled_query = (
        to_blocks(probe_vectors.reshape(span_tokens, parallel_groups, head_key)).astype(jnp.float32)
        * query_scale
    )
    readout = jnp.einsum("bchk,bhkv->bchv", scaled_query, states).reshape(
        span_tokens, parallel_groups, value_part
    )
    gated_grad = jnp.dot(
        stream_full,
        result_mapping_matrix.reshape(model_width, parallel_groups * value_part),
        preferred_element_type=jnp.float32,
    ).reshape(span_tokens, parallel_groups, value_part)
    gate_value = result_valve_scores.astype(jnp.float32)
    gate_silu = jax.nn.silu(gate_value)
    gated_flat = (
        (readout * gate_silu)
        .astype(jnp.bfloat16)
        .reshape(span_tokens, parallel_groups * value_part)
    )
    product = lax.dot_general(
        stream_full, gated_flat, (((0,), (0,)), ((), ())), preferred_element_type=jnp.float32
    )
    proj_grad = sum_at_owner(
        product.reshape(
            model_width // sp_count * lax.axis_size(SP), parallel_groups, value_part
        ).astype(jnp.bfloat16),
        SP,
        0,
    )
    readout_grad = gated_grad * gate_silu
    gate_input_grad = (gated_grad * readout * silu_slope(gate_value)).astype(jnp.bfloat16)
    readout_blocks = to_blocks(readout_grad)
    local_terms = jnp.einsum("bchk,bchv->bhkv", scaled_query, readout_blocks)
    carried = jnp.zeros_like(running_state)
    local_list = [carried] * blocks
    for block_index in reversed(range(blocks)):
        local_list[block_index] = local_terms[block_index] + carried
        carried = local_list[block_index] * jnp.exp(totals[block_index])[:, :, None]
    local_grads = jnp.stack(local_list)
    span_total = jnp.sum(totals, axis=0)
    span_decay = jnp.exp(span_total)
    identity = (jnp.ones_like(span_decay), jnp.zeros_like(carried))
    scanned = carried_in((span_decay, carried), SP, chain_join, identity)
    incoming = scanned[1]
    tail_sum = span_total[None] - jnp.cumsum(totals, axis=0)
    state_grad = local_grads + jnp.exp(tail_sum)[..., None] * incoming[None]
    value_grad = (
        jnp.einsum("bchk,bhkv->bchv", decayed.astype(jnp.float32), state_grad)
        .astype(jnp.bfloat16)
        .reshape(span_tokens, parallel_groups, value_part)
    )
    decayed_grad = jnp.einsum("bchv,bhkv->bchk", value_blocks.astype(jnp.float32), state_grad)
    combined_derivative = jnp.sum(priors * jnp.exp(totals)[..., None] * state_grad, axis=3)
    query_part = (jnp.einsum("bchv,bhkv->bchk", readout_blocks, states) * query_scale).astype(
        jnp.bfloat16
    )
    query_grad = sum_at_owner(query_part.reshape(span_tokens, key_width), "tp", 1).astype(
        jnp.bfloat16
    )
    key_sums, total_sums = tuple(
        (
            part.astype(jnp.float32)
            for part in sum_packed(
                (
                    decayed_grad.reshape(span_tokens, key_width).astype(jnp.bfloat16),
                    combined_derivative.reshape(blocks, key_width).astype(jnp.bfloat16),
                ),
                "tp",
                (1, 1),
            )
        )
    )
    own_width = key_width // tp_count
    own_start = tp_index * own_width

    def own_columns(tensor):
        return lax.dynamic_slice_in_dim(
            tensor.reshape(span_tokens, key_width), own_start, own_width, 1
        )

    key_grad = (key_sums * own_columns(factor)).astype(jnp.bfloat16)
    moved_terms = (key_sums * own_columns(key_weight)).reshape(blocks, PIECE_PLACES, own_width)
    preceding_cumulation = jnp.cumsum(moved_terms, axis=1) - moved_terms
    logit_own = own_columns(persistence_scores.astype(jnp.float32))
    retain_preact_derivative = (
        (total_sums[:, None] + preceding_cumulation).reshape(span_tokens, own_width)
        * jax.nn.sigmoid(-logit_own)
        / toggle_smoothness
    )
    return (
        stream_grad,
        gate_grad,
        up_grad,
        down_grad,
        proj_grad,
        query_grad,
        key_grad,
        retain_preact_derivative,
        value_grad,
        gate_input_grad,
    )


def solution(mesh):
    finer = Mesh(mesh.devices.reshape(16, 2, mesh.shape["tp"]), ("sp_0", "sp_1", "tp"))
    in_specs = (
        P(SP_TP, None),
        P(),
        P(SP_TP, None),
        P(SP, None),
        P(SP, None),
        P(SP, None, "tp"),
        P(SP, None, "tp"),
        P(SP, "tp", None),
        P(SP, None),
        P(SP, None),
        P(SP, None),
        P(SP, None),
        P(SP, None, "tp"),
        P(SP, None, "tp"),
        P(SP, None, None, "tp"),
        P(None, None, "tp"),
    )
    out_specs = (
        P(SP_TP, None),
        P(SP, None, "tp"),
        P(SP, None, "tp"),
        P(SP, "tp", None),
        P(SP, None, "tp"),
        P(SP, "tp"),
        P(SP, "tp"),
        P(SP, "tp"),
        P(SP, None, "tp"),
        P(SP, None, "tp"),
    )
    return jax.shard_map(
        on_device, mesh=finer, in_specs=in_specs, out_specs=out_specs, check_vma=False
    )
```

profile of v0, /device:TPU:1, one launch (start us, length us, event | category | flops | bytes accessed | tf_op | source)
XLA Modules:
  0.0 418.8 jit_solution(11178201702546347338)
XLA Ops:
  9.2 7.6 %all-to-all-start = ((bf16[16,8,2,2048]{3,1,2,0:T(8,128)(2,1)}), bf16[16,8,2,2048]{3,1,2,0:T(8,128)(2,1)S(1)}, u32[]{:S(2)}, u32[]{:S(2)}) async-start(bf16[16,8,2,2048]{3,1,2,0:T(8,128)(2,1)} %broadcast_in_dim.20), calls=%async_computation | async-start | bytes 2097152 | tf_op jit(solution)/shard_map/all_to_all | solution.py:18
  20.2 11.2 %all-to-all-done = bf16[16,8,2,2048]{3,1,2,0:T(8,128)(2,1)S(1)} async-done(((bf16[16,8,2,2048]{3,1,2,0:T(8,128)(2,1)}), bf16[16,8,2,2048]{3,1,2,0:T(8,128)(2,1)S(1)}, u32[]{:S(2)}, u32[]{:S(2)}) %all-to-all-start) | async-done | bytes 1048608 | tf_op jit(solution)/shard_map/all_to_all | solution.py:18
  33.7 2.6 mul.465
  36.2 3.7 mul.466
  44.1 36.2 %all_to_all.40 = bf16[32,10,2,128]{3,2,1,0:T(2,128)(2,1)S(1)} all-to-all(bf16[32,10,2,128]{3,2,1,0:T(2,128)(2,1)S(1)} %copy.182), channel_id=1, replica_groups=mesh['sp_0'=16,'sp_1'=2,'tp'=16] {'sp_0','sp_1'}, dimensions={0} | all-to-all | bytes 327680 | tf_op jit(solution)/shard_map/all_to_all | solution.py:185
  81.0 35.4 %all_to_all.41 = bf16[16,32,10,2,128]{4,1,3,2,0:T(8,128)(2,1)S(1)} all-to-all(bf16[16,32,10,2,128]{4,1,3,2,0:T(8,128)(2,1)S(1)} %broadcast_in_dim.24), channel_id=1, replica_groups=mesh['sp_0'=16,'sp_1'=2,'tp'=16] {'tp'}, dimensions={0} | all-to-all | bytes 5242880 | tf_op jit(solution)/shard_map/all_to_all | solution.py:18
  116.4 3.2 copy.184
  119.6 5.3 %reshape_transpose_reshape_reshape.3 = bf16[1,320,2,2048]{3,1,2,0:T(8,128)(2,1)} reshape(bf16[32,10,2,16,128]{4,3,1,0,2:T(8,128)(2,1)} %copy.184) | data formatting | bytes 5242880 | tf_op jit(solution)/shard_map/reshape;transpose;reshape;reshape | solution.py:190
  132.3 4.0 all-to-all-start.3
  140.2 3.8 all-gather.1
  144.0 9.7 %all-to-all-done.3 = bf16[16,32,10,128]{3,1,2,0:T(8,128)(2,1)S(1)} async-done(((bf16[16,32,10,128]{3,1,2,0:T(8,128)(2,1)}), bf16[16,32,10,128]{3,1,2,0:T(8,128)(2,1)S(1)}, u32[]{:S(2)}, u32[]{:S(2)}) %all-to-all-start.3) | async-done | bytes 1310752 | tf_op jit(solution)/shard_map/all_to_all | solution.py:40
  154.6 10.2 %all-to-all-start.4 = ((bf16[32,10,128]{2,1,0:T(8,128)(2,1)}), bf16[32,10,128]{2,1,0:T(8,128)(2,1)S(1)}, u32[]{:S(2)}, u32[]{:S(2)}) async-start(bf16[32,10,128]{2,1,0:T(8,128)(2,1)} %copy.186), calls=%async_computation.4 | async-start | bytes 262144 | tf_op jit(solution)/shard_map/all_to_all | solution.py:199
  166.5 14.1 %all-to-all-done.4 = bf16[32,10,128]{2,1,0:T(8,128)(2,1)S(1)} async-done(((bf16[32,10,128]{2,1,0:T(8,128)(2,1)}), bf16[32,10,128]{2,1,0:T(8,128)(2,1)S(1)}, u32[]{:S(2)}, u32[]{:S(2)}) %all-to-all-start.4) | async-done | bytes 81952 | tf_op jit(solution)/shard_map/all_to_all | solution.py:199
  182.6 3.6 all-to-all-start.5
  190.0 6.2 %all-to-all-done.5 = bf16[16,128,128]{2,1,0:T(8,128)(2,1)S(1)} async-done(((bf16[16,128,128]{2,1,0:T(8,128)(2,1)}), bf16[16,128,128]{2,1,0:T(8,128)(2,1)S(1)}, u32[]{:S(2)}, u32[]{:S(2)}) %all-to-all-start.5) | async-done | bytes 524320 | tf_op jit(solution)/shard_map/all_to_all | solution.py:18
  205.4 4.0 all_gather.16
  212.9 21.7 %all_gather.19 = bf16[16,2,512]{2,1,0:T(2,128)(2,1)} all-gather(bf16[1,2,512]{2,1,0:T(2,128)(2,1)S(1)} %get-tuple-element.95), channel_id=1, replica_groups=mesh['sp_0'=16,'sp_1'=2,'tp'=16] {'sp_0'}, dimensions={0}, use_global_device_ids=true | all-gather | bytes 34816 | tf_op jit(solution)/shard_map/all_gather | solution.py:56
  236.6 4.2 %all-to-all-start.7 = ((bf16[16,128,64]{1,2,0:T(8,128)(2,1)}), bf16[16,128,64]{1,2,0:T(8,128)(2,1)}, u32[]{:S(2)}, u32[]{:S(2)}) async-start(bf16[16,128,64]{1,2,0:T(8,128)(2,1)} %copy.199), calls=%async_computation.7 | async-start | bytes 524288 | tf_op jit(solution)/shard_map/all_to_all | solution.py:40
  244.2 4.2 %all-to-all-done.7 = bf16[16,128,64]{1,2,0:T(8,128)(2,1)} async-done(((bf16[16,128,64]{1,2,0:T(8,128)(2,1)}), bf16[16,128,64]{1,2,0:T(8,128)(2,1)}, u32[]{:S(2)}, u32[]{:S(2)}) %all-to-all-start.7) | async-done | bytes 262176 | tf_op jit(solution)/shard_map/all_to_all | solution.py:40
  248.3 13.9 %all-to-all-start.6 = ((bf16[32,2,4096]{2,1,0:T(2,128)(2,1)}), bf16[32,2,4096]{2,1,0:T(2,128)(2,1)}, u32[]{:S(2)}, u32[]{:S(2)}) async-start(bf16[32,2,4096]{2,1,0:T(2,128)(2,1)} %reshape.625), calls=%async_computation.6 | async-start | bytes 1048576 | tf_op jit(solution)/shard_map/all_to_all | solution.py:40
  275.6 2.3 fusion.1
  284.9 10.5 %all-to-all-done.6 = bf16[32,2,4096]{2,1,0:T(2,128)(2,1)} async-done(((bf16[32,2,4096]{2,1,0:T(2,128)(2,1)}), bf16[32,2,4096]{2,1,0:T(2,128)(2,1)}, u32[]{:S(2)}, u32[]{:S(2)}) %all-to-all-start.6) | async-done | bytes 524320 | tf_op jit(solution)/shard_map/all_to_all | solution.py:40
  298.0 2.3 add_bitcast_fusion
  307.7 99.2 %all-reduce.6.cloned.1.call-done = bf16[1152,128]{1,0:T(8,128)(2,1)} async-done(((bf16[1152,128]{1,0:T(8,128)(2,1)}), bf16[1152,128]{1,0:T(8,128)(2,1)}) %all-reduce.6.cloned.1.call-update) | async-done | bytes 294928
  (269 shorter events, 83.7 us)
Async XLA Ops:
  7.2 117.7 %copy-start = (bf16[1,2048,128]{2,1,0:T(8,128)(2,1)S(1)}, bf16[1,2048,128]{2,1,0:T(8,128)(2,1)}, u32[]{:S(2)}) copy-start(bf16[1,2048,128]{2,1,0:T(8,128)(2,1)} %param.21) | copy-start | bytes 1572868
  9.2 22.2 %all-to-all-start = ((bf16[16,8,2,2048]{3,1,2,0:T(8,128)(2,1)}), bf16[16,8,2,2048]{3,1,2,0:T(8,128)(2,1)S(1)}, u32[]{:S(2)}, u32[]{:S(2)}) async-start(bf16[16,8,2,2048]{3,1,2,0:T(8,128)(2,1)} %broadcast_in_dim.20), calls=%async_computation | async-start | bytes 2097152 | tf_op jit(solution)/shard_map/all_to_all | solution.py:18
  32.9 169.4 %copy-start.58 = (f32[128]{0:T(128)}, f32[128]{0:T(128)S(1)}, u32[]{:S(2)}) copy-start(f32[128]{0:T(128)S(1)} %add_rsqrt_fusion) | copy-start | bytes 1540
  132.3 21.3 %all-to-all-start.3 = ((bf16[16,32,10,128]{3,1,2,0:T(8,128)(2,1)}), bf16[16,32,10,128]{3,1,2,0:T(8,128)(2,1)S(1)}, u32[]{:S(2)}, u32[]{:S(2)}) async-start(bf16[16,32,10,128]{3,1,2,0:T(8,128)(2,1)} %bitcast.283), calls=%async_computation.3 | async-start | bytes 2621440 | tf_op jit(solution)/shard_map/all_to_all | solution.py:40
  153.9 35.0 %copy-start.4 = (f32[16,8,16,128]{3,1,2,0:T(8,128)S(1)}, f32[16,8,16,128]{3,1,2,0:T(8,128)}, u32[]{:S(2)}) copy-start(f32[16,8,16,128]{3,1,2,0:T(8,128)} %get-tuple-element.66) | copy-start | bytes 3145732
  154.6 26.1 %all-to-all-start.4 = ((bf16[32,10,128]{2,1,0:T(8,128)(2,1)}), bf16[32,10,128]{2,1,0:T(8,128)(2,1)S(1)}, u32[]{:S(2)}, u32[]{:S(2)}) async-start(bf16[32,10,128]{2,1,0:T(8,128)(2,1)} %copy.186), calls=%async_computation.4 | async-start | bytes 262144 | tf_op jit(solution)/shard_map/all_to_all | solution.py:199
  182.6 13.7 %all-to-all-start.5 = ((bf16[16,128,128]{2,1,0:T(8,128)(2,1)}), bf16[16,128,128]{2,1,0:T(8,128)(2,1)S(1)}, u32[]{:S(2)}, u32[]{:S(2)}) async-start(bf16[16,128,128]{2,1,0:T(8,128)(2,1)} %broadcast_in_dim.25), calls=%async_computation.5 | async-start | bytes 1048576 | tf_op jit(solution)/shard_map/all_to_all | solution.py:18
  186.2 111.6 %all-gather.4.cloned.1.call-start = ((), (), s32[]{:S(2)}) async-start(), calls=%async_computation.8 | async-start | bytes 2228224 | tf_op jit(solution)/shard_map/all_gather | solution.py:56
  186.2 23.2 %copy-start.34 = (f32[2,512]{1,0:T(2,128)}, f32[2,512]{1,0:T(2,128)S(1)}, u32[]{:S(2)}) copy-start(f32[2,512]{1,0:T(2,128)S(1)} %fusion.95) | copy-start | bytes 12292
  188.1 21.3 %copy-start.36 = (f32[2,512]{1,0:T(2,128)}, f32[2,512]{1,0:T(2,128)S(1)}, u32[]{:S(2)}) copy-start(f32[2,512]{1,0:T(2,128)S(1)} %get-tuple-element.96) | copy-start | bytes 12292
  212.1 23.0 %copy-start.15 = (bf16[2,64,2,512]{3,2,1,0:T(2,128)(2,1)}, bf16[2,64,2,512]{3,2,1,0:T(2,128)(2,1)S(1)}, u32[]{:S(2)}) copy-start(bf16[2,64,2,512]{3,2,1,0:T(2,128)(2,1)S(1)} %get-tuple-element.64) | copy-start | bytes 786436
  212.4 24.2 %copy-start.8 = (f32[1,2,512,64]{2,3,1,0:T(8,128)}, f32[1,2,512,64]{2,3,1,0:T(8,128)S(1)}, u32[]{:S(2)}) copy-start(f32[1,2,512,64]{2,3,1,0:T(8,128)S(1)} %get-tuple-element.63) | copy-start | bytes 786436
  212.6 28.2 %copy-start.23 = (bf16[128,2,64]{0,2,1:T(8,128)(2,1)S(1)}, bf16[128,2,64]{0,2,1:T(8,128)(2,1)}, u32[]{:S(2)}) copy-start(bf16[128,2,64]{0,2,1:T(8,128)(2,1)} %param.29) | copy-start | bytes 98308
  236.6 11.7 %all-to-all-start.7 = ((bf16[16,128,64]{1,2,0:T(8,128)(2,1)}), bf16[16,128,64]{1,2,0:T(8,128)(2,1)}, u32[]{:S(2)}, u32[]{:S(2)}) async-start(bf16[16,128,64]{1,2,0:T(8,128)(2,1)} %copy.199), calls=%async_computation.7 | async-start | bytes 524288 | tf_op jit(solution)/shard_map/all_to_all | solution.py:40
  244.2 31.4 %copy-start.2 = (bf16[1,320,2,2048]{3,1,2,0:T(8,128)(2,1)S(1)}, bf16[1,320,2,2048]{3,1,2,0:T(8,128)(2,1)}, u32[]{:S(2)}) copy-start(bf16[1,320,2,2048]{3,1,2,0:T(8,128)(2,1)} %reshape_transpose_reshape_reshape.3) | copy-start | bytes 7864324
  248.3 47.1 %all-to-all-start.6 = ((bf16[32,2,4096]{2,1,0:T(2,128)(2,1)}), bf16[32,2,4096]{2,1,0:T(2,128)(2,1)}, u32[]{:S(2)}, u32[]{:S(2)}) async-start(bf16[32,2,4096]{2,1,0:T(2,128)(2,1)} %reshape.625), calls=%async_computation.6 | async-start | bytes 1048576 | tf_op jit(solution)/shard_map/all_to_all | solution.py:40
  262.2 144.7 %all-reduce.6.cloned.1.call-start = ((), (), s32[]{:S(2)}) async-start(), calls=%async_computation.9 | async-start | bytes 589824
  280.7 17.0 %copy-start.42 = (f32[2,512]{1,0:T(2,128)S(1)}, f32[2,512]{1,0:T(2,128)}, u32[]{:S(2)}) copy-start(f32[2,512]{1,0:T(2,128)} %get-tuple-element.80) | copy-start | bytes 12292
  280.8 17.0 %copy-start.43 = (f32[2,512]{1,0:T(2,128)S(1)}, f32[2,512]{1,0:T(2,128)}, u32[]{:S(2)}) copy-start(f32[2,512]{1,0:T(2,128)} %get-tuple-element.81) | copy-start | bytes 12292
  280.8 17.0 %copy-start.44 = (f32[2,512]{1,0:T(2,128)S(1)}, f32[2,512]{1,0:T(2,128)}, u32[]{:S(2)}) copy-start(f32[2,512]{1,0:T(2,128)} %get-tuple-element.82) | copy-start | bytes 12292
  280.8 17.0 %copy-start.45 = (f32[2,512]{1,0:T(2,128)S(1)}, f32[2,512]{1,0:T(2,128)}, u32[]{:S(2)}) copy-start(f32[2,512]{1,0:T(2,128)} %get-tuple-element.83) | copy-start | bytes 12292
  280.8 17.0 %copy-start.46 = (f32[2,512]{1,0:T(2,128)S(1)}, f32[2,512]{1,0:T(2,128)}, u32[]{:S(2)}) copy-start(f32[2,512]{1,0:T(2,128)} %get-tuple-element.84) | copy-start | bytes 12292
  280.8 17.0 %copy-start.47 = (f32[2,512]{1,0:T(2,128)S(1)}, f32[2,512]{1,0:T(2,128)}, u32[]{:S(2)}) copy-start(f32[2,512]{1,0:T(2,128)} %get-tuple-element.85) | copy-start | bytes 12292
  280.8 17.0 %copy-start.48 = (f32[2,512]{1,0:T(2,128)S(1)}, f32[2,512]{1,0:T(2,128)}, u32[]{:S(2)}) copy-start(f32[2,512]{1,0:T(2,128)} %get-tuple-element.86) | copy-start | bytes 12292
  (49 other events, 406.0 us)
Sparse Core Ops, SparseCore 0:
  210.3 50.9 all-gather.3
  304.9 101.9 all-reduce.5
where the time goes:
time: 421 us; the launch traced here: 419 us
  waiting for transfers between devices  155 us (37%)
  blocking collectives  101 us (24%)
  local copies, waits for them, and re-layouts  56.1 us (13%)
  starting transfers between devices  43.8 us (10%)
  other arithmetic  32.6 us (8%)
  between operations  16 us (4%)
  matrix products  14 us (3%)
    unnamed x3, waiting for transfers between devices  99.3 us
    all_to_all x1, blocking collectives, on_device(): lax.all_to_all(outgoing, SP, split_axis=0, concat_axis=0, tiled=True)  36.2 us
    all_to_all x1, blocking collectives, from_everyone(): return lax.all_to_all(copies, axis, split_axis=0, concat_axis=0, tiled=True)  35.4 us
    all_gather x3, blocking collectives, carried_in(): lax.all_gather(part.astype(kind), axis)  29.5 us
    all_to_all x3, waiting for transfers between devices, sum_at_owner(): lax.all_to_all(cut_along(shard, dim, length), axis, 0, 0, tiled=True)  24.4 us
    all_to_all x3, starting transfers between devices, sum_at_owner(): lax.all_to_all(cut_along(shard, dim, length), axis, 0, 0, tiled=True)  22.1 us
    all_to_all x2, waiting for transfers between devices, from_everyone(): return lax.all_to_all(copies, axis, split_axis=0, concat_axis=0, tiled=True)  17.4 us
    all_to_all x1, waiting for transfers between devices, on_device(): lax.all_to_all(summed, SP, split_axis=0, concat_axis=0, tiled=True)  14.1 us
  transfers between devices with their start and end apart: 8, of which 7 were waited for; matrix products, arithmetic and copies ran while one was open for 11% of the time, Pallas kernels for 0%

commit v1 on v0

--- a/solution.py
+++ b/solution.py
@@ -41,40 +41,31 @@
     return jnp.sum(tiles.astype(jnp.float32), axis=0)
 
 
-def filled_with(shard, identity):
-    return jax.tree.map(
-        lambda a, e: jnp.broadcast_to(jnp.asarray(e, a.dtype), a.shape), shard, identity
-    )
-
-
-def carried_in(shard, axes, combine, identity):
-    before = start = filled_with(shard, identity)
-    total = shard
-    for axis in reversed(axes):
-        length, index = (lax.axis_size(axis), lax.axis_index(axis))
-        pieces = jax.tree.map(
-            lambda part, kind: lax.all_gather(part.astype(kind), axis),
-            total,
-            (jnp.bfloat16, jnp.bfloat16),
-        )
-        inside, total = (start, start)
-        for k in reversed(range(length)):
-            passed = k > index
-            total = combine(
-                total, jax.tree.map(lambda part, own: part[k].astype(own.dtype), pieces, shard)
-            )
-            inside = jax.tree.map(lambda new, old: jnp.where(passed, new, old), total, inside)
-        before = combine(inside, before)
-    return before
+def carried_in(decay, carried):
+    length = lax.axis_size(SP)
+    shape = carried.shape
+    mine = shape[0] * shape[1] // length
+    decays = lax.all_gather(decay.reshape(-1), SP)
+    start = lax.axis_index(SP) * mine
+    decays = lax.dynamic_slice_in_dim(decays, start, mine, 1)
+    pieces = carried.astype(jnp.bfloat16).reshape(length, mine, shape[2])
+    pieces = lax.all_to_all(pieces, SP, 0, 0, tiled=True).astype(jnp.float32)
+    value = jnp.zeros_like(pieces[0])
+    values = [value] * length
+    for k in reversed(range(length - 1)):
+        value = pieces[k + 1] + decays[k + 1][:, None] * value
+        values[k] = value
+    values = jnp.stack(values).astype(jnp.bfloat16)
+    back = lax.all_to_all(values, SP, 0, 0, tiled=True)
+    return back.reshape(shape).astype(jnp.float32)
 
 
 def sum_packed(arrays, axis, dims):
     length = lax.axis_size(axis)
     tiles = [cut_along(a, dim, length) for a, dim in zip(arrays, dims)]
-    lines = jnp.concatenate([b.reshape(length, -1) for b in tiles], axis=1)
-    extent = max(16, -(-lines.shape[1] // 1024) * 8)
-    lines = jnp.pad(lines, ((0, 0), (0, extent * 128 - lines.shape[1]))).reshape(-1, 128)
-    line, at, gathered = (lax.psum_scatter(lines, axis, tiled=True).reshape(-1), 0, [])
+    lines = jnp.concatenate([b.reshape(length, -1, 128) for b in tiles], axis=1)
+    line = jnp.sum(lax.all_to_all(lines, axis, 0, 0, tiled=True).astype(jnp.float32), axis=0)
+    line, at, gathered = (line.reshape(-1), 0, [])
     for b in tiles:
         part = b[0]
         gathered.append(line[at : at + part.size].reshape(part.shape))
@@ -85,13 +76,6 @@
 def silu_slope(value):
     sigma = jax.nn.sigmoid(value)
     return sigma + value * sigma * (1.0 - sigma)
-
-
-def chain_join(first_part, second_part):
-    return (
-        first_part[0] * second_part[0],
-        second_part[1] + second_part[0][..., None] * first_part[1],
-    )
 
 
 def expert_backward(routed_rows, w_gate, w_up, w_down):
@@ -146,14 +130,16 @@
     own_rows = residual_signal.shape[0]
     model_width = residual_signal.shape[1]
     column_width = model_width // tp_count
-    paired = jnp.stack([residual_signal, result_adjoint], axis=1)
-    span_pair = gather_directly(paired, "tp", 0)
-    residual = span_pair[:, 0].astype(jnp.float32)
-    cotangent = span_pair[:, 1]
-    span_tokens = residual.shape[0]
-    inv_rms = lax.rsqrt(jnp.mean(residual * residual, axis=1, keepdims=True) + norm_eps)
-    unit_rows = residual * inv_rms
-    moe_input = (unit_rows * prelayer_scaling_factor).astype(jnp.bfloat16)
+    own_residual = residual_signal.astype(jnp.float32)
+    inv_rms = lax.rsqrt(jnp.mean(own_residual * own_residual, axis=1, keepdims=True) + norm_eps)
+    unit_rows = own_residual * inv_rms
+    own_input = (unit_rows * prelayer_scaling_factor).astype(jnp.bfloat16)
+    paired = jnp.stack([cut_along(own_input, 1, tp_count), cut_along(result_adjoint, 1, tp_count)], axis=2)
+    paired = lax.all_to_all(paired.reshape(tp_count, own_rows, 2 * column_width), "tp", 0, 0, tiled=True)
+    paired = paired.reshape(tp_count * own_rows, 2 * column_width)
+    input_table = paired[:, :column_width]
+    cotangent = paired[:, column_width:]
+    span_tokens = paired.shape[0]
     top_count = chosen_specialist_ids.shape[1]
     weighted = (dispatch_shares[:, :, None] * cotangent.astype(jnp.float32)[:, None, :]).astype(
         jnp.bfloat16
@@ -173,17 +159,16 @@
         .at[destination]
         .set(jnp.arange(assigned, dtype=jnp.int32))
     )
-    input_table = moe_input
-    cot_table = weighted.reshape(assigned, model_width)
-    input_table = lax.dynamic_slice_in_dim(input_table, tp_index * column_width, column_width, 1)
-    cot_table = lax.dynamic_slice_in_dim(cot_table, tp_index * column_width, column_width, 1)
-    send_width = input_table.shape[1]
-    input_table = jnp.concatenate([input_table, jnp.zeros((1, send_width), jnp.bfloat16)], axis=0)
-    cot_table = jnp.concatenate([cot_table, jnp.zeros((1, send_width), jnp.bfloat16)], axis=0)
-    outgoing = jnp.stack([input_table[source_of // top_count], cot_table[source_of]], axis=1)
-    outgoing = outgoing.reshape(expert_total, capacity, 2, send_width)
+    cot_table = weighted.reshape(assigned, column_width)
+    input_table = jnp.concatenate([input_table, jnp.zeros((1, column_width), jnp.bfloat16)], axis=0)
+    cot_table = jnp.concatenate([cot_table, jnp.zeros((1, column_width), jnp.bfloat16)], axis=0)
+    outgoing = jnp.concatenate([input_table[source_of // top_count], cot_table[source_of]], axis=1)
+    outgoing = outgoing.reshape(expert_total, capacity, 2 * column_width)
     arrived = lax.all_to_all(outgoing, SP, split_axis=0, concat_axis=0, tiled=True)
-    arrived = gather_directly(arrived, "tp", 3)
+    arrived = from_everyone(arrived, "tp").reshape(
+        tp_count, sp_count * capacity, 2, column_width
+    )
+    arrived = jnp.transpose(arrived, (1, 2, 0, 3)).reshape(sp_count, capacity, 2, model_width)
     by_expert = jnp.moveaxis(
         arrived.reshape(sp_count, local_experts, capacity, 2, model_width), 1, 0
     )
@@ -201,15 +186,16 @@
         jnp.float32
     )
     grad_columns = jnp.sum(picked.reshape(span_tokens, top_count, column_width), axis=1)
-    input_grad = gather_directly(grad_columns.astype(jnp.bfloat16), "tp", 1).astype(
-        grad_columns.dtype
-    )
+    input_grad = lax.all_to_all(
+        grad_columns.astype(jnp.bfloat16).reshape(tp_count, own_rows, column_width), "tp", 0, 0, tiled=True
+    )
+    input_grad = joined_along(input_grad, 1).astype(jnp.float32)
     scaled = prelayer_scaling_factor * input_grad
-    stream_full = (
-        cotangent.astype(jnp.float32)
+    stream_grad = (
+        result_adjoint.astype(jnp.float32)
         + inv_rms * (scaled - unit_rows * jnp.mean(scaled * unit_rows, axis=1, keepdims=True))
     ).astype(jnp.bfloat16)
-    stream_grad = lax.dynamic_slice_in_dim(stream_full, tp_index * own_rows, own_rows, 0)
+    stream_full = gather_directly(stream_grad, "tp", 0)
     parallel_groups = group_additional_shrinkage.shape[1]
     key_width = probe_vectors.shape[1]
     head_key = key_width // parallel_groups
@@ -293,9 +279,7 @@
     local_grads = jnp.stack(local_list)
     span_total = jnp.sum(totals, axis=0)
     span_decay = jnp.exp(span_total)
-    identity = (jnp.ones_like(span_decay), jnp.zeros_like(carried))
-    scanned = carried_in((span_decay, carried), SP, chain_join, identity)
-    incoming = scanned[1]
+    incoming = carried_in(span_decay, carried)
     tail_sum = span_total[None] - jnp.cumsum(totals, axis=0)
     state_grad = local_grads + jnp.exp(tail_sum)[..., None] * incoming[None]
     value_grad = (

time: 421 us -> 406 us (0.964)
  waiting for transfers between devices: 155 us -> 47.9 us
  other arithmetic: 32.6 us -> 68.6 us
  local copies, waits for them, and re-layouts: 56.1 us -> 82.1 us
  starting transfers between devices: 43.8 us -> 68.5 us
  between operations: 16 us -> 1.3 us
  blocking collectives: 101 us -> 112 us
  matrix products: 14 us -> 22.7 us
    unnamed x3 -> x0, waiting for transfers between devices: 99.3 us -> none
    all_to_all x0 -> x5, starting transfers between devices: none -> 35.7 us  [the longest x1 12.3 us: carried_in(): pieces = lax.all_to_all(pieces, SP, 0, 0, tiled=True).astype(jnp.float32)]
    unnamed x2 -> x31, other arithmetic: 1.23 us -> 29.1 us
    all_to_all x0 -> x5, waiting for transfers between devices: none -> 16.8 us  [the longest x1 10.7 us: carried_in(): pieces = lax.all_to_all(pieces, SP, 0, 0, tiled=True).astype(jnp.float32)]
    all_to_all x1, waiting for transfers between devices: 14.1 us -> 0.01 us  [on_device(): lax.all_to_all(summed, SP, split_axis=0, concat_axis=0, tiled=True)]
    all_to_all x2 -> x1, waiting for transfers between devices: 17.4 us -> 6.54 us  [from_everyone(): return lax.all_to_all(copies, axis, split_axis=0, concat_axis=0, tiled=True)]
    unnamed x141 -> x70, local copies, waits for them, and re-layouts: 13.2 us -> 20.2 us
    mul x3 -> x2, local copies, waits for them, and re-layouts: 6.35 us -> 0.18 us  [on_device(): dispatch_shares[:, :, None] * cotangent.astype(jnp.float32)[:, None, :]]
  transfers between devices with their start and end apart: 8 -> 10, of which waited for: 7 -> 6; matrix products, arithmetic and copies ran while one was open for 11% -> 23% of each run, Pallas kernels for 0% -> 0%
where the time goes in v1:
time: 406 us; the launch traced here: 403 us
  blocking collectives  112 us (28%)
  local copies, waits for them, and re-layouts  82.1 us (20%)
  other arithmetic  68.6 us (17%)
  starting transfers between devices  68.5 us (17%)
  waiting for transfers between devices  47.9 us (12%)
  matrix products  22.7 us (6%)
    all_to_all x1, blocking collectives, on_device(): lax.all_to_all(outgoing, SP, split_axis=0, concat_axis=0, tiled=True)  39.4 us
    all_to_all x1, blocking collectives, from_everyone(): return lax.all_to_all(copies, axis, split_axis=0, concat_axis=0, tiled=True)  37.3 us
    all_gather x1, blocking collectives, carried_in(): decays = lax.all_gather(decay.reshape(-1), SP)  35.2 us
    unnamed x31, other arithmetic  29.1 us
    all_to_all x3, waiting for transfers between devices, sum_at_owner(): lax.all_to_all(cut_along(shard, dim, length), axis, 0, 0, tiled=True)  24.5 us
    unnamed x70, local copies, waits for them, and re-layouts  20.2 us
    all_to_all x3, starting transfers between devices, sum_at_owner(): lax.all_to_all(cut_along(shard, dim, length), axis, 0, 0, tiled=True)  16.6 us
    all_to_all x1, starting transfers between devices, carried_in(): pieces = lax.all_to_all(pieces, SP, 0, 0, tiled=True).astype(jnp.float32)  12.3 us
  transfers between devices with their start and end apart: 10, of which 6 were waited for; matrix products, arithmetic and copies ran while one was open for 23% of the time, Pallas kernels for 0%

profile of v1, /device:TPU:1, one launch (start us, length us, event | category | flops | bytes accessed | tf_op | source)
XLA Modules:
  0.0 403.1 jit_solution(2687101814227587595)
XLA Ops:
  3.9 7.6 %all-to-all-start = ((bf16[16,8,256]{2,1,0:T(8,128)(2,1)}), bf16[16,8,256]{2,1,0:T(8,128)(2,1)S(1)}, u32[]{:S(2)}, u32[]{:S(2)}) async-start(bf16[16,8,256]{2,1,0:T(8,128)(2,1)} %copy_bitcast_fusion.1), calls=%async_computation | async-start | bytes 131072 | tf_op jit(solution)/shard_map/all_to_all | solution.py:138
  21.1 39.4 %all_to_all.60 = bf16[32,10,256]{2,1,0:T(8,128)(2,1)S(1)} all-to-all(bf16[32,10,256]{2,1,0:T(8,128)(2,1)S(1)} %reshape.3273), channel_id=1, replica_groups=mesh['sp_0'=16,'sp_1'=2,'tp'=16] {'sp_0','sp_1'}, dimensions={0} | all-to-all | bytes 327680 | tf_op jit(solution)/shard_map/all_to_all | solution.py:167
  60.9 37.3 %all_to_all.61 = bf16[16,32,10,256]{3,1,2,0:T(8,128)(2,1)S(1)} all-to-all(bf16[16,32,10,256]{3,1,2,0:T(8,128)(2,1)S(1)} %broadcast_in_dim.15), channel_id=1, replica_groups=mesh['sp_0'=16,'sp_1'=2,'tp'=16] {'tp'}, dimensions={0} | all-to-all | bytes 5242880 | tf_op jit(solution)/shard_map/all_to_all | solution.py:18
  99.7 2.8 reshape.3274
  104.6 3.1 reshape_transpose_reshape_reshape.3
  115.4 4.5 %all-to-all-start.3 = ((bf16[16,32,10,128]{3,1,2,0:T(8,128)(2,1)}), bf16[16,32,10,128]{3,1,2,0:T(8,128)(2,1)}, u32[]{:S(2)}, u32[]{:S(2)}) async-start(bf16[16,32,10,128]{3,1,2,0:T(8,128)(2,1)} %bitcast.243), calls=%async_computation.3 | async-start | bytes 2621440 | tf_op jit(solution)/shard_map/all_to_all | solution.py:40
  126.2 11.5 %all-to-all-done.3 = bf16[16,32,10,128]{3,1,2,0:T(8,128)(2,1)} async-done(((bf16[16,32,10,128]{3,1,2,0:T(8,128)(2,1)}), bf16[16,32,10,128]{3,1,2,0:T(8,128)(2,1)}, u32[]{:S(2)}, u32[]{:S(2)}) %all-to-all-start.3) | async-done | bytes 1310752 | tf_op jit(solution)/shard_map/all_to_all | solution.py:40
  139.9 9.5 %all-to-all-start.4 = ((bf16[32,10,128]{2,1,0:T(8,128)(2,1)}), bf16[32,10,128]{2,1,0:T(8,128)(2,1)}, u32[]{:S(2)}, u32[]{:S(2)}) async-start(bf16[32,10,128]{2,1,0:T(8,128)(2,1)} %copy.194), calls=%async_computation.4 | async-start | bytes 262144 | tf_op jit(solution)/shard_map/all_to_all | solution.py:184
  150.0 35.2 %all-gather = f32[32,1,1024]{2,1,0:T(1,128)} all-gather(f32[1,1,1024]{2,1,0:T(1,128)S(1)} %reshape.3330), channel_id=1, replica_groups=mesh['sp_0'=16,'sp_1'=2,'tp'=16] {'sp_0','sp_1'}, dimensions={0}, use_global_device_ids=true | all-gather | bytes 135168 | tf_op jit(solution)/shard_map/all_gather | solution.py:48
  189.6 3.5 all-to-all-start.5
  203.5 6.7 %all-to-all-start.6 = ((bf16[16,8,2048]{2,1,0:T(8,128)(2,1)}), bf16[16,8,2048]{2,1,0:T(8,128)(2,1)}, u32[]{:S(2)}, u32[]{:S(2)}) async-start(bf16[16,8,2048]{2,1,0:T(8,128)(2,1)} %broadcast_in_dim.16), calls=%async_computation.6 | async-start | bytes 1048576 | tf_op jit(solution)/shard_map/all_to_all | solution.py:18
  210.2 2.5 multiply_convert_fusion.1
  214.4 6.5 %all-to-all-done.6 = bf16[16,8,2048]{2,1,0:T(8,128)(2,1)} async-done(((bf16[16,8,2048]{2,1,0:T(8,128)(2,1)}), bf16[16,8,2048]{2,1,0:T(8,128)(2,1)}, u32[]{:S(2)}, u32[]{:S(2)}) %all-to-all-start.6) | async-done | bytes 524320 | tf_op jit(solution)/shard_map/all_to_all | solution.py:18
  232.7 12.3 %all-to-all-start.9 = ((bf16[32,2,1024]{2,1,0:T(2,128)(2,1)}), bf16[32,2,1024]{2,1,0:T(2,128)(2,1)}, u32[]{:S(2)}, u32[]{:S(2)}) async-start(bf16[32,2,1024]{2,1,0:T(2,128)(2,1)} %reshape.3412), calls=%async_computation.9 | async-start | bytes 262144 | tf_op jit(solution)/shard_map/all_to_all | solution.py:52
  250.3 10.7 %all-to-all-done.9 = bf16[32,2,1024]{2,1,0:T(2,128)(2,1)} async-done(((bf16[32,2,1024]{2,1,0:T(2,128)(2,1)}), bf16[32,2,1024]{2,1,0:T(2,128)(2,1)}, u32[]{:S(2)}, u32[]{:S(2)}) %all-to-all-start.9) | async-done | bytes 131104 | tf_op jit(solution)/shard_map/all_to_all | solution.py:52
  295.3 5.7 %all-to-all-start.10 = ((bf16[32,2,1024]{2,1,0:T(2,128)(2,1)}), bf16[32,2,1024]{2,1,0:T(2,128)(2,1)}, u32[]{:S(2)}, u32[]{:S(2)}) async-start(bf16[32,2,1024]{2,1,0:T(2,128)(2,1)} %reshape.3414), calls=%async_computation.10 | async-start | bytes 262144 | tf_op jit(solution)/shard_map/all_to_all | solution.py:59
  312.3 5.0 %all-to-all-done.10 = bf16[32,2,1024]{2,1,0:T(2,128)(2,1)} async-done(((bf16[32,2,1024]{2,1,0:T(2,128)(2,1)}), bf16[32,2,1024]{2,1,0:T(2,128)(2,1)}, u32[]{:S(2)}, u32[]{:S(2)}) %all-to-all-start.10) | async-done | bytes 131104 | tf_op jit(solution)/shard_map/all_to_all | solution.py:59
  317.3 4.2 %all-to-all-start.8 = ((bf16[16,128,64]{1,2,0:T(8,128)(2,1)}), bf16[16,128,64]{1,2,0:T(8,128)(2,1)}, u32[]{:S(2)}, u32[]{:S(2)}) async-start(bf16[16,128,64]{1,2,0:T(8,128)(2,1)} %copy.204), calls=%async_computation.8 | async-start | bytes 524288 | tf_op jit(solution)/shard_map/all_to_all | solution.py:40
  341.2 6.6 %all-to-all-start.11 = ((bf16[16,65,128]{2,1,0:T(8,128)(2,1)}), bf16[16,65,128]{2,1,0:T(8,128)(2,1)}, u32[]{:S(2)}, u32[]{:S(2)}) async-start(bf16[16,65,128]{2,1,0:T(8,128)(2,1)} %pad_maximum_fusion.3), calls=%async_computation.11 | async-start | bytes 589824 | tf_op jit(solution)/shard_map/all_to_all | solution.py:67
  350.0 2.8 reshape.3285
  352.8 2.6 copy.249
  355.4 3.0 reshape.3410
  358.4 7.9 %all-to-all-start.7 = ((bf16[32,2,4096]{2,1,0:T(2,128)(2,1)}), bf16[32,2,4096]{2,1,0:T(2,128)(2,1)}, u32[]{:S(2)}, u32[]{:S(2)}) async-start(bf16[32,2,4096]{2,1,0:T(2,128)(2,1)} %reshape.3410), calls=%async_computation.7 | async-start | bytes 1048576 | tf_op jit(solution)/shard_map/all_to_all | solution.py:40
  386.8 13.0 %all-to-all-done.7 = bf16[32,2,4096]{2,1,0:T(2,128)(2,1)} async-done(((bf16[32,2,4096]{2,1,0:T(2,128)(2,1)}), bf16[32,2,4096]{2,1,0:T(2,128)(2,1)}, u32[]{:S(2)}, u32[]{:S(2)}) %all-to-all-start.7) | async-done | bytes 524320 | tf_op jit(solution)/shard_map/all_to_all | solution.py:40
  (222 shorter events, 157.8 us)
Async XLA Ops:
  0.6 107.1 %copy-start = (bf16[1,2048,128]{2,1,0:T(8,128)(2,1)S(1)}, bf16[1,2048,128]{2,1,0:T(8,128)(2,1)}, u32[]{:S(2)}) copy-start(bf16[1,2048,128]{2,1,0:T(8,128)(2,1)} %param.21) | copy-start | bytes 1572868
  1.6 9.8 %copy-start.24 = (f32[8]{0:T(128)}, f32[8]{0:T(128)S(1)}, u32[]{:S(2)}) copy-start(f32[8]{0:T(128)S(1)} %add_rsqrt_fusion) | copy-start | bytes 100
  3.9 14.1 %all-to-all-start = ((bf16[16,8,256]{2,1,0:T(8,128)(2,1)}), bf16[16,8,256]{2,1,0:T(8,128)(2,1)S(1)}, u32[]{:S(2)}, u32[]{:S(2)}) async-start(bf16[16,8,256]{2,1,0:T(8,128)(2,1)} %copy_bitcast_fusion.1), calls=%async_computation | async-start | bytes 131072 | tf_op jit(solution)/shard_map/all_to_all | solution.py:138
  113.8 6.1 %copy-start.5 = (bf16[128,1024]{1,0:T(8,128)(2,1)S(1)}, bf16[128,1024]{1,0:T(8,128)(2,1)}, u32[]{:S(2)}) copy-start(bf16[128,1024]{1,0:T(8,128)(2,1)} %param.26) | copy-start | bytes 786436
  115.4 7.9 %copy-start.26 = (f32[128,2]{0,1:T(2,128)S(1)}, f32[128,2]{0,1:T(2,128)}, u32[]{:S(2)}) copy-start(f32[128,2]{0,1:T(2,128)} %param.27) | copy-start | bytes 3076
  115.4 22.3 %all-to-all-start.3 = ((bf16[16,32,10,128]{3,1,2,0:T(8,128)(2,1)}), bf16[16,32,10,128]{3,1,2,0:T(8,128)(2,1)}, u32[]{:S(2)}, u32[]{:S(2)}) async-start(bf16[16,32,10,128]{3,1,2,0:T(8,128)(2,1)} %bitcast.243), calls=%async_computation.3 | async-start | bytes 2621440 | tf_op jit(solution)/shard_map/all_to_all | solution.py:40
  123.4 73.1 %copy-start.4 = (bf16[128,1024]{1,0:T(8,128)(2,1)S(1)}, bf16[128,1024]{1,0:T(8,128)(2,1)}, u32[]{:S(2)}) copy-start(bf16[128,1024]{1,0:T(8,128)(2,1)} %param.25) | copy-start | bytes 786436
  125.6 61.4 %copy-start.21 = (f32[2,512]{1,0:T(2,128)}, f32[2,512]{1,0:T(2,128)S(1)}, u32[]{:S(2)}) copy-start(f32[2,512]{1,0:T(2,128)S(1)} %get-tuple-element.84) | copy-start | bytes 12292
  139.9 47.1 %all-to-all-start.4 = ((bf16[32,10,128]{2,1,0:T(8,128)(2,1)}), bf16[32,10,128]{2,1,0:T(8,128)(2,1)}, u32[]{:S(2)}, u32[]{:S(2)}) async-start(bf16[32,10,128]{2,1,0:T(8,128)(2,1)} %copy.194), calls=%async_computation.4 | async-start | bytes 262144 | tf_op jit(solution)/shard_map/all_to_all | solution.py:184
  189.6 11.1 %all-to-all-start.5 = ((bf16[16,8,128]{2,1,0:T(8,128)(2,1)}), bf16[16,8,128]{2,1,0:T(8,128)(2,1)S(1)}, u32[]{:S(2)}, u32[]{:S(2)}) async-start(bf16[16,8,128]{2,1,0:T(8,128)(2,1)} %bitcast.20), calls=%async_computation.5 | async-start | bytes 65536 | tf_op jit(solution)/shard_map/all_to_all | solution.py:189
  197.8 23.1 %copy-start.11 = (bf16[128,2,64]{0,2,1:T(8,128)(2,1)S(1)}, bf16[128,2,64]{0,2,1:T(8,128)(2,1)}, u32[]{:S(2)}) copy-start(bf16[128,2,64]{0,2,1:T(8,128)(2,1)} %param.29) | copy-start | bytes 98308
  202.6 20.4 %copy-start.18 = (bf16[8,2048]{1,0:T(8,128)(2,1)}, bf16[8,2048]{1,0:T(8,128)(2,1)S(1)}, u32[]{:S(2)}) copy-start(bf16[8,2048]{1,0:T(8,128)(2,1)S(1)} %fusion.47) | copy-start | bytes 98308
  203.5 20.4 %copy-start.7 = (bf16[2,64,2,512]{3,2,1,0:T(2,128)(2,1)S(1)}, bf16[2,64,2,512]{3,2,1,0:T(2,128)(2,1)}, u32[]{:S(2)}) copy-start(bf16[2,64,2,512]{3,2,1,0:T(2,128)(2,1)} %mul.972) | copy-start | bytes 786436
  203.5 17.4 %all-to-all-start.6 = ((bf16[16,8,2048]{2,1,0:T(8,128)(2,1)}), bf16[16,8,2048]{2,1,0:T(8,128)(2,1)}, u32[]{:S(2)}, u32[]{:S(2)}) async-start(bf16[16,8,2048]{2,1,0:T(8,128)(2,1)} %broadcast_in_dim.16), calls=%async_computation.6 | async-start | bytes 1048576 | tf_op jit(solution)/shard_map/all_to_all | solution.py:18
  223.9 8.8 %copy-start.8 = (bf16[2,64,2,64]{1,0,3,2:T(2,128)(2,1)}, bf16[2,64,2,64]{1,0,3,2:T(2,128)(2,1)S(1)}, u32[]{:S(2)}) copy-start(bf16[2,64,2,64]{1,0,3,2:T(2,128)(2,1)S(1)} %reshape.3287) | copy-start | bytes 98308
  230.9 32.9 %copy-start.25 = (f32[32]{0:T(128)S(1)}, f32[32]{0:T(128)}, u32[]{:S(2)}) copy-start(f32[32]{0:T(128)} %get-tuple-element.93) | copy-start | bytes 388
  232.7 28.2 %all-to-all-start.9 = ((bf16[32,2,1024]{2,1,0:T(2,128)(2,1)}), bf16[32,2,1024]{2,1,0:T(2,128)(2,1)}, u32[]{:S(2)}, u32[]{:S(2)}) async-start(bf16[32,2,1024]{2,1,0:T(2,128)(2,1)} %reshape.3412), calls=%async_computation.9 | async-start | bytes 262144 | tf_op jit(solution)/shard_map/all_to_all | solution.py:52
  247.7 57.3 %copy-start.22 = (f32[2,512]{1,0:T(2,128)S(1)}, f32[2,512]{1,0:T(2,128)}, u32[]{:S(2)}) copy-start(f32[2,512]{1,0:T(2,128)} %copy-done.21) | copy-start | bytes 12292
  295.3 22.0 %all-to-all-start.10 = ((bf16[32,2,1024]{2,1,0:T(2,128)(2,1)}), bf16[32,2,1024]{2,1,0:T(2,128)(2,1)}, u32[]{:S(2)}, u32[]{:S(2)}) async-start(bf16[32,2,1024]{2,1,0:T(2,128)(2,1)} %reshape.3414), calls=%async_computation.10 | async-start | bytes 262144 | tf_op jit(solution)/shard_map/all_to_all | solution.py:59
  305.8 21.3 %copy-start.23 = (f32[2,2,512]{2,1,0:T(2,128)S(1)}, f32[2,2,512]{2,1,0:T(2,128)}, u32[]{:S(2)}) copy-start(f32[2,2,512]{2,1,0:T(2,128)} %fusion.109) | copy-start | bytes 24580
  317.3 24.0 %all-to-all-start.8 = ((bf16[16,128,64]{1,2,0:T(8,128)(2,1)}), bf16[16,128,64]{1,2,0:T(8,128)(2,1)}, u32[]{:S(2)}, u32[]{:S(2)}) async-start(bf16[16,128,64]{1,2,0:T(8,128)(2,1)} %copy.204), calls=%async_computation.8 | async-start | bytes 524288 | tf_op jit(solution)/shard_map/all_to_all | solution.py:40
  332.4 15.4 %copy-start.12 = (bf16[128,2,64]{0,2,1:T(8,128)(2,1)S(1)}, bf16[128,2,64]{0,2,1:T(8,128)(2,1)}, u32[]{:S(2)}) copy-start(bf16[128,2,64]{0,2,1:T(8,128)(2,1)} %param.29) | copy-start | bytes 98308
  341.2 17.1 %all-to-all-start.11 = ((bf16[16,65,128]{2,1,0:T(8,128)(2,1)}), bf16[16,65,128]{2,1,0:T(8,128)(2,1)}, u32[]{:S(2)}, u32[]{:S(2)}) async-start(bf16[16,65,128]{2,1,0:T(8,128)(2,1)} %pad_maximum_fusion.3), calls=%async_computation.11 | async-start | bytes 589824 | tf_op jit(solution)/shard_map/all_to_all | solution.py:67
  358.4 41.5 %all-to-all-start.7 = ((bf16[32,2,4096]{2,1,0:T(2,128)(2,1)}), bf16[32,2,4096]{2,1,0:T(2,128)(2,1)}, u32[]{:S(2)}, u32[]{:S(2)}) async-start(bf16[32,2,4096]{2,1,0:T(2,128)(2,1)} %reshape.3410), calls=%async_computation.7 | async-start | bytes 1048576 | tf_op jit(solution)/shard_map/all_to_all | solution.py:40
  (14 other events, 30.7 us)

commit v2 on v1

v2 whole, which is shorter than its diff:
```python
import jax
import jax.numpy as jnp
from jax import lax
from jax.experimental import pallas as pl
from jax.experimental.pallas import tpu as pltpu
from jax.sharding import PartitionSpec as P

MESH = pl.DeviceIdType.MESH
F32 = jnp.float32
BF16 = jnp.bfloat16
HIGHEST = lax.Precision.HIGHEST

BLOCK = 64
TOGGLE = 16.0
EPS = 1e-06
PITCH = 16


def iota(shape, dim):
    return lax.broadcasted_iota(jnp.int32, shape, dim)


def dot(a, b):
    return jnp.dot(a, b, preferred_element_type=F32)


def dot_nt(a, b):
    return lax.dot_general(a, b, (((1,), (1,)), ((), ())), preferred_element_type=F32)


def dot_tn(a, b):
    return lax.dot_general(a, b, (((0,), (0,)), ((), ())), preferred_element_type=F32)


def silu_slope(value, sigma):
    return sigma + value * sigma * (1.0 - sigma)


def peer(me, i, n):
    half = n // 2
    up = half - i // 2
    offset = jnp.where(i % 2 == 0, up, n - up + 1)
    return lax.rem(me + offset, n)


def kernel(
    n_sp,
    n_tp,
    cap,
    res_ref,
    cot_ref,
    gain_ref,
    ids_row_ref,
    share_ref,
    wg_ref,
    wu_ref,
    wd_ref,
    q_ref,
    k_ref,
    pers_ref,
    shrink_ref,
    val_ref,
    valve_ref,
    mem_ref,
    map_ref,
    stream_out,
    gate_out,
    up_out,
    down_out,
    proj_out,
    query_out,
    key_out,
    retain_out,
    value_out,
    gig_out,
    p0_send,
    p0_recv,
    dec_all,
    p1_send,
    p1_recv,
    cx,
    cw,
    x_all,
    w_all,
    wgu,
    rs_send,
    rs_recv,
    ret_send,
    ret_recv,
    ig_send,
    ig_recv,
    st_send,
    st_recv,
    sc_send,
    sc_recv,
    bk_send,
    bk_recv,
    pj_local,
    pj_away,
    pj_partner,
    pj_send,
    pj_recv,
    q_send,
    q_recv,
    k_send,
    k_recv,
    m_sum,
    factor_ref,
    kw_ref,
    states,
    readout_ref,
    local_ref,
    sf_ref,
    gup_ref,
    hid_ref,
    ssem,
    rsem,
):
    sp = lax.axis_index("sp")
    tp = lax.axis_index("tp")
    core = lax.rem(sp, 2)
    own_rows, width = res_ref.shape
    tokens = own_rows * n_tp
    rows = n_sp * cap
    padded = n_sp * PITCH
    head_k = q_ref.shape[1] // 2

    barrier = pltpu.get_barrier_semaphore()

    def greet(axis, me, n):
        def body(i, carry):
            pl.semaphore_signal(
                barrier, inc=1, device_id={axis: peer(me, i, n)}, device_id_type=MESH
            )
            return carry

        lax.fori_loop(0, n - 1, body, 0)

    greet("sp", sp, n_sp)
    greet("tp", tp, n_tp)

    def copy(src, dst, slot, device):
        return pltpu.make_async_remote_copy(
            src_ref=src,
            dst_ref=dst,
            send_sem=ssem.at[slot],
            recv_sem=rsem.at[slot],
            device_id=device,
            device_id_type=MESH,
        )

    def spread(axis, me, n, slot, src_of, dst):
        def body(i, carry):
            p = peer(me, i, n)
            copy(src_of(p), dst, slot, {axis: p}).start()
            return carry

        lax.fori_loop(0, n - 1, body, 0)

    def received(slot, part):
        copy(part, part, slot, {"tp": lax.rem(tp + 1, n_tp)}).wait_recv()

    def sent(slot, part):
        copy(part, part, slot, {"tp": lax.rem(tp + 1, n_tp)}).wait_send()

    residual = res_ref[...].astype(F32)
    own_cot = cot_ref[...]
    inv_rms = lax.rsqrt(jnp.mean(residual * residual, axis=1, keepdims=True) + EPS)
    unit = residual * inv_rms
    own_input = (unit * gain_ref[...]).astype(BF16)
    for j in range(n_tp):
        p0_send[j, :, 0:128] = own_input[:, 128 * j : 128 * (j + 1)]
        p0_send[j, :, 128:256] = own_cot[:, 128 * j : 128 * (j + 1)]
    p0_recv[tp] = p0_send[tp]

    pl.semaphore_wait(barrier, (n_sp - 1) + (n_tp - 1))
    spread("tp", tp, n_tp, 0, lambda p: p0_send.at[p], p0_recv.at[tp])

    spot = iota((padded, tokens), 0)
    expert_rows = iota((n_sp, tokens), 0)
    earlier = (iota((tokens, tokens), 0) < iota((tokens, tokens), 1)).astype(BF16)
    ids0 = ids_row_ref[0:1, :]
    ids1 = ids_row_ref[1:2, :]
    hot0 = (expert_rows == ids0).astype(F32)
    hot1 = (expert_rows == ids1).astype(F32)
    counts = dot((hot0 + hot1).astype(BF16), earlier)
    slot0 = jnp.sum(hot0 * counts, axis=0, keepdims=True).astype(jnp.int32)
    slot1 = jnp.sum(hot1 * counts, axis=0, keepdims=True).astype(jnp.int32)
    pick0 = (spot == ids0 * PITCH + slot0).astype(F32).astype(BF16)
    pick1 = (spot == ids1 * PITCH + slot1).astype(F32).astype(BF16)
    m_sum[...] = pick0 + pick1

    received(0, p0_recv.at[pl.ds(0, n_tp - 1)])
    table = p0_recv[...].astype(F32).reshape(tokens, 256)
    cot_table = table[:, 128:256]
    weighted0 = (share_ref[:, 0:1] * cot_table).astype(BF16)
    weighted1 = (share_ref[:, 1:2] * cot_table).astype(BF16)
    p1_send[:, :, 0:128] = (
        dot(m_sum[...], table[:, 0:128].astype(BF16)).astype(BF16).reshape(n_sp, PITCH, 128)
    )
    p1_send[:, :, 128:256] = (
        (dot(pick0, weighted0) + dot(pick1, weighted1)).astype(BF16).reshape(n_sp, PITCH, 128)
    )
    p1_recv[sp] = p1_send[sp]
    spread("sp", sp, n_sp, 1, lambda p: p1_send.at[p], p1_recv.at[sp])

    log_decay = pers_ref[...].astype(F32)
    log_decay = (jnp.minimum(log_decay, 0.0) - jnp.log1p(jnp.exp(-jnp.abs(log_decay)))) / TOGGLE
    left = iota((tokens, 2 * head_k), 1) < head_k
    log_decay = log_decay + jnp.where(left, shrink_ref[:, 0:1], shrink_ref[:, 1:2])
    row_id = iota((tokens, tokens), 0)
    col_id = iota((tokens, tokens), 1)
    after = ((col_id > row_id) & (col_id // BLOCK == row_id // BLOCK)).astype(F32)
    factor = jnp.exp(
        jnp.dot(after, log_decay, preferred_element_type=F32, precision=HIGHEST)
    )
    factor_ref[...] = factor
    total0 = jnp.sum(log_decay[0:BLOCK], axis=0, keepdims=True)
    total1 = jnp.sum(log_decay[BLOCK : 2 * BLOCK], axis=0, keepdims=True)
    etot0 = jnp.exp(total0)
    etot1 = jnp.exp(total1)
    span_decay = jnp.exp(total0 + total1)
    for j in range(8):
        dec_all[sp, j : j + 1, :] = span_decay[:, 128 * j : 128 * (j + 1)]
    spread("sp", sp, n_sp, 2, lambda p: dec_all.at[sp], dec_all.at[sp])
    key_weight = k_ref[...].astype(F32) * factor
    kw_ref[...] = key_weight
    wgu[:, 0:128] = wg_ref[...]
    wgu[:, 128:256] = wu_ref[...]

    received(1, p1_recv.at[pl.ds(0, n_sp - 1)])
    r_i = iota((rows, padded), 0)
    q_i = iota((rows, padded), 1)
    tight = ((q_i & (PITCH - 1)) < cap) & (r_i == (q_i // PITCH) * cap + (q_i & (PITCH - 1)))
    tight = tight.astype(F32).astype(BF16)
    compact = dot(tight, p1_recv[...].reshape(padded, 256)).astype(BF16)
    cx[...] = compact[:, 0:128]
    cw[...] = compact[:, 128:256]
    own_lanes = pl.ds(pl.multiple_of(tp * 128, 128), 128)
    spread("tp", tp, n_tp, 3, lambda p: cx, x_all.at[:, own_lanes])
    spread("tp", tp, n_tp, 4, lambda p: cw, w_all.at[:, own_lanes])
    x_all[:, own_lanes] = compact[:, 0:128]
    w_all[:, own_lanes] = compact[:, 128:256]

    scale = float(head_k) ** (-0.5)
    decayed = key_weight.astype(BF16)
    values_t = val_ref[...].astype(F32).T
    tok_block = iota((128, tokens), 1) // BLOCK
    etots = (etot0, etot1)
    for b in range(2):
        masked = jnp.where(tok_block == b, values_t, 0.0).astype(BF16)
        for h in range(2):
            term = dot(masked[64 * h : 64 * (h + 1)], decayed[:, head_k * h : head_k * (h + 1)])
            if b == 0:
                prior = mem_ref[64 * h : 64 * (h + 1), :]
            else:
                prior = states[0, 64 * h : 64 * (h + 1), :]
            states[b, 64 * h : 64 * (h + 1), :] = (
                prior * etots[b][:, head_k * h : head_k * (h + 1)] + term
            )
    first_head = iota((BLOCK, 128), 1) < 64

    def per_head(a, m, b):
        part = [
            dot_nt(a[BLOCK * b : BLOCK * (b + 1), head_k * h : head_k * (h + 1)], m)
            for h in range(2)
        ]
        return jnp.where(first_head, part[0], part[1])

    for b in range(2):
        readout_ref[BLOCK * b : BLOCK * (b + 1), :] = (
            per_head(q_ref[...], states[b].astype(BF16), b) * scale
        )

    received(3, x_all.at[:, pl.ds(0, 128 * (n_tp - 1))])
    received(4, w_all.at[:, pl.ds(0, 128 * (n_tp - 1))])
    pre = dot(x_all[...], wgu[...])
    pre_gate = pre[:, 0:128]
    pre_up = pre[:, 128:256]
    hidden_grad = dot_nt(w_all[...], wd_ref[...])
    sigma = jax.nn.sigmoid(pre_gate)
    silu = pre_gate * sigma
    gup_ref[:, 0:128] = (hidden_grad * pre_up * silu_slope(pre_gate, sigma)).astype(BF16)
    gup_ref[:, 128:256] = (hidden_grad * silu).astype(BF16)
    hid_ref[...] = (silu * pre_up).astype(BF16)

    def partial_of(p):
        return dot_nt(
            gup_ref[...], wgu[pl.ds(pl.multiple_of(p * 128, 128), 128), :]
        ).astype(BF16)

    def send_partial(i, carry):
        p = peer(tp, i, n_tp)
        rs_send[p] = partial_of(p)
        copy(rs_send.at[p], rs_recv.at[tp], 5, {"tp": p}).start()
        return carry

    lax.fori_loop(0, n_tp - 1, send_partial, 0)
    rs_recv[tp] = partial_of(tp)

    for j in range(width // 256):
        lanes = slice(256 * j, 256 * (j + 1))
        both = dot_tn(x_all[:, lanes], gup_ref[...])
        gate_out[lanes, :] = both[:, 0:128].astype(BF16)
        up_out[lanes, :] = both[:, 128:256].astype(BF16)
    down_out[...] = dot_tn(hid_ref[...], w_all[...]).astype(BF16)

    received(5, rs_recv.at[pl.ds(0, n_tp - 1)])
    summed = rs_recv[0].astype(F32)
    for j in range(1, n_tp):
        summed = summed + rs_recv[j].astype(F32)
    q_i = iota((padded, rows), 0)
    r_i = iota((padded, rows), 1)
    loose = ((q_i & (PITCH - 1)) < cap) & (r_i == (q_i // PITCH) * cap + (q_i & (PITCH - 1)))
    loose = loose.astype(F32).astype(BF16)
    ret_send[...] = dot(loose, summed.astype(BF16)).astype(BF16).reshape(n_sp, PITCH, 128)
    ret_recv[sp] = ret_send[sp]
    spread("sp", sp, n_sp, 6, lambda p: ret_send.at[p], ret_recv.at[sp])
    received(6, ret_recv.at[pl.ds(0, n_sp - 1)])

    picked = dot_tn(m_sum[...], ret_recv[...].reshape(padded, 128))
    ig_send[...] = picked.reshape(n_tp, own_rows, 128).astype(BF16)
    ig_recv[tp] = ig_send[tp]
    spread("tp", tp, n_tp, 7, lambda p: ig_send.at[p], ig_recv.at[tp])
    received(7, ig_recv.at[pl.ds(0, n_tp - 1)])
    input_grad = jnp.concatenate([ig_recv[j].astype(F32) for j in range(n_tp)], axis=1)
    scaled = gain_ref[...] * input_grad
    stream = (
        own_cot.astype(F32)
        + inv_rms * (scaled - unit * jnp.mean(scaled * unit, axis=1, keepdims=True))
    ).astype(BF16)
    stream_out[...] = stream
    st_send[...] = stream
    st_recv[tp] = stream
    spread("tp", tp, n_tp, 8, lambda p: st_send, st_recv.at[tp])
    received(8, st_recv.at[pl.ds(0, n_tp - 1)])
    sf_ref[...] = st_recv[...].astype(F32).reshape(tokens, width).astype(BF16)

    gated_grad = dot(sf_ref[...], map_ref[...])
    gate_value = valve_ref[...].astype(F32)
    gate_sigma = jax.nn.sigmoid(gate_value)
    gate_silu = gate_value * gate_sigma
    readout_grad = gated_grad * gate_silu
    rg = readout_grad.astype(BF16)
    rg_t = readout_grad.T
    for b in range(1, -1, -1):
        masked = jnp.where(tok_block == b, rg_t, 0.0).astype(BF16)
        for h in range(2):
            hs = slice(64 * h, 64 * (h + 1))
            ks = slice(head_k * h, head_k * (h + 1))
            term = dot(masked[hs], q_ref[:, ks]) * scale
            if b == 0:
                term = term + local_ref[1, hs, :] * etot1[:, ks]
            local_ref[b, hs, :] = term
            if b == 0:
                out = (term * etot0[:, ks]).astype(BF16)
                for r in range(4):
                    for c in range(4):
                        sc_send[(4 * h + r) * 4 + c] = out[
                            16 * r : 16 * (r + 1), 128 * c : 128 * (c + 1)
                        ]
    sc_recv[sp] = sc_send[sp]
    spread("sp", sp, n_sp, 9, lambda p: sc_send.at[p], sc_recv.at[sp])

    readout = readout_ref[...]
    gig_out[...] = (gated_grad * readout * silu_slope(gate_value, gate_sigma)).astype(BF16)
    gated = (readout * gate_silu).astype(BF16)
    partner = sp + 1 - 2 * core
    for j in range(width // 256):
        lanes = slice(256 * j, 256 * (j + 1))
        part = dot_tn(sf_ref[:, lanes], gated).astype(BF16)
        for i in range(2):
            z = 2 * j + i
            lower = part[128 * i : 128 * i + 64]
            upper = part[128 * i + 64 : 128 * i + 128]
            pj_local[z] = jnp.where(core == 0, lower, upper)
            pj_away[z] = jnp.where(core == 0, upper, lower)
    copy(pj_away, pj_partner, 10, {"sp": partner}).start()

    lower_lanes = iota((BLOCK, 128), 1) < 64

    def swap(a):
        return jnp.concatenate([a[:, 64:128], a[:, 0:64]], axis=1)

    def even_of(a, b):
        return jnp.where(lower_lanes[0 : a.shape[0]], a, swap(b))

    def odd_of(a, b):
        return jnp.where(lower_lanes[0 : a.shape[0]], swap(a), b)

    def by_head(a, m, h):
        keep = first_head if h == 0 else jnp.logical_not(first_head)
        return dot(jnp.where(keep, a.astype(F32), 0.0).astype(BF16), m)

    for h in range(2):
        part = [
            by_head(rg[BLOCK * b : BLOCK * (b + 1)], states[b].astype(BF16), h) * scale
            for b in range(2)
        ]
        for m in range(4):
            ls = slice(128 * m, 128 * (m + 1))
            q_send[8 * h + 2 * m] = even_of(part[0][:, ls], part[1][:, ls]).astype(BF16)
            q_send[8 * h + 2 * m + 1] = odd_of(part[0][:, ls], part[1][:, ls]).astype(BF16)
    q_recv[tp] = q_send[tp]
    spread("tp", tp, n_tp, 11, lambda p: q_send.at[p], q_recv.at[tp])

    received(2, dec_all.at[pl.ds(0, n_sp - 1)])
    received(9, sc_recv.at[pl.ds(0, n_sp - 1)])
    group = (sp // 16) * 4 + lax.rem(sp, 4)
    run = jnp.zeros((16, 128), F32)
    bk_send[n_sp - 1] = run.astype(BF16)
    for s in range(n_sp - 1, 0, -1):
        run = sc_recv[s].astype(F32) + dec_all[s, pl.ds(group, 1), :] * run
        bk_send[s - 1] = run.astype(BF16)
    bk_recv[sp] = bk_send[sp]
    spread("sp", sp, n_sp, 12, lambda p: bk_send.at[p], bk_recv.at[sp])

    received(10, pj_partner)
    pj_send[...] = (pj_local[...].astype(F32) + pj_partner[...].astype(F32)).astype(BF16)
    chip = sp // 2
    n_z = n_sp // 2

    def send_proj(i, carry):
        p = peer(chip, i, n_z)
        copy(pj_send.at[p], pj_recv.at[chip], 13, {"sp": 2 * p + core}).start()
        return carry

    lax.fori_loop(0, n_z - 1, send_proj, 0)
    pj_recv[chip] = pj_send[chip]

    received(12, bk_recv.at[pl.ds(0, n_sp - 1)])
    incoming = jnp.concatenate(
        [
            jnp.concatenate([bk_recv[4 * r + c].astype(F32) for c in range(4)], axis=1)
            for r in range(8)
        ],
        axis=0,
    )
    weight = jnp.concatenate(
        [
            jnp.broadcast_to(etot1[:, 0:head_k], (64, head_k)),
            jnp.broadcast_to(etot1[:, head_k : 2 * head_k], (64, head_k)),
        ],
        axis=0,
    )
    local_ref[1] = local_ref[1] + incoming
    local_ref[0] = local_ref[0] + weight * incoming
    grads = [local_ref[b].astype(BF16) for b in range(2)]
    for h in range(2):
        part = [
            by_head(val_ref[BLOCK * b : BLOCK * (b + 1), :], grads[b], h) for b in range(2)
        ]
        sums = []
        for b in range(2):
            hs = slice(64 * h, 64 * (h + 1))
            prior = mem_ref[hs, :] if b == 0 else states[0, hs, :]
            sums.append(
                jnp.sum(prior * local_ref[b, hs, :], axis=0, keepdims=True)
                * etots[b][:, head_k * h : head_k * (h + 1)]
            )
        for m in range(4):
            ls = slice(128 * m, 128 * (m + 1))
            for odd, of in ((0, even_of), (1, odd_of)):
                p = 8 * h + 2 * m + odd
                k_send[p, 0:BLOCK, :] = of(part[0][:, ls], part[1][:, ls]).astype(BF16)
                k_send[p, BLOCK : BLOCK + 16, :] = jnp.broadcast_to(
                    of(sums[0][:, ls], sums[1][:, ls]), (16, 128)
                ).astype(BF16)
    k_recv[tp] = k_send[tp]
    spread("tp", tp, n_tp, 14, lambda p: k_send.at[p], k_recv.at[tp])

    decayed = kw_ref[...].astype(BF16)
    for b in range(2):
        value_out[BLOCK * b : BLOCK * (b + 1), :] = per_head(decayed, grads[b], b).astype(BF16)

    def two_blocks(out, a):
        out[0:BLOCK, :] = a[:, 0:64].astype(out.dtype)
        out[BLOCK : 2 * BLOCK, :] = a[:, 64:128].astype(out.dtype)

    received(11, q_recv.at[pl.ds(0, n_tp - 1)])
    query = q_recv[0].astype(F32)
    for j in range(1, n_tp):
        query = query + q_recv[j].astype(F32)
    two_blocks(query_out, query)

    lanes = pl.ds(pl.multiple_of((tp // 2) * 128, 128), 128)
    is_odd = lax.rem(tp, 2) == 1

    def own_columns(ref):
        a = ref[0:BLOCK, lanes].astype(F32)
        b = ref[BLOCK : 2 * BLOCK, lanes].astype(F32)
        return jnp.where(is_odd, odd_of(a, b), even_of(a, b))

    own_factor = own_columns(factor_ref)
    own_weight = own_columns(kw_ref)
    slope = jax.nn.sigmoid(-own_columns(pers_ref)) / TOGGLE
    before = (iota((BLOCK, BLOCK), 0) > iota((BLOCK, BLOCK), 1)).astype(F32)

    received(14, k_recv.at[pl.ds(0, n_tp - 1)])
    keys = k_recv[0].astype(F32)
    for j in range(1, n_tp):
        keys = keys + k_recv[j].astype(F32)
    key_sum = keys[0:BLOCK]
    two_blocks(key_out, key_sum * own_factor)
    preceding = jnp.dot(
        before, key_sum * own_weight, preferred_element_type=F32, precision=HIGHEST
    )
    two_blocks(retain_out, (keys[BLOCK : BLOCK + 1] + preceding) * slope)

    received(13, pj_recv.at[pl.ds(0, n_z - 1)])
    proj = pj_recv[0].astype(F32)
    for j in range(1, n_z):
        proj = proj + pj_recv[j].astype(F32)
    proj_out[...] = proj

    sent(0, p0_send.at[pl.ds(0, n_tp - 1)])
    sent(1, p1_send.at[pl.ds(0, n_sp - 1)])
    sent(2, dec_all.at[pl.ds(0, n_sp - 1)])
    sent(3, x_all.at[:, pl.ds(0, 128 * (n_tp - 1))])
    sent(4, w_all.at[:, pl.ds(0, 128 * (n_tp - 1))])
    sent(5, rs_send.at[pl.ds(0, n_tp - 1)])
    sent(6, ret_send.at[pl.ds(0, n_sp - 1)])
    sent(7, ig_send.at[pl.ds(0, n_tp - 1)])
    sent(8, st_recv.at[pl.ds(0, n_tp - 1)])
    sent(9, sc_send.at[pl.ds(0, n_sp - 1)])
    sent(10, pj_away)
    sent(11, q_send.at[pl.ds(0, n_tp - 1)])
    sent(12, bk_send.at[pl.ds(0, n_sp - 1)])
    sent(13, pj_send.at[pl.ds(0, n_z - 1)])
    sent(14, k_send.at[pl.ds(0, n_tp - 1)])


def on_device(
    residual_signal,
    prelayer_scaling_factor,
    result_adjoint,
    chosen_specialist_ids,
    dispatch_shares,
    specialist_valve_matrix,
    specialist_widen_matrix,
    specialist_shrink_matrix,
    probe_vectors,
    lookup_vectors,
    persistence_scores,
    group_additional_shrinkage,
    content_vectors,
    result_valve_scores,
    stored_opening_memory,
    result_mapping_matrix,
):
    n_sp = lax.axis_size("sp")
    n_tp = lax.axis_size("tp")
    own_rows, width = residual_signal.shape
    tokens = own_rows * n_tp
    assigned = tokens * chosen_specialist_ids.shape[1]
    cap = assigned // n_sp + assigned // (4 * n_sp)
    rows = n_sp * cap
    padded = n_sp * PITCH
    head_k = probe_vectors.shape[1] // 2
    n_z = n_sp // 2

    args = (
        residual_signal,
        result_adjoint,
        prelayer_scaling_factor.reshape(1, width),
        chosen_specialist_ids.T,
        dispatch_shares,
        specialist_valve_matrix[0],
        specialist_widen_matrix[0],
        specialist_shrink_matrix[0],
        probe_vectors,
        lookup_vectors,
        persistence_scores,
        group_additional_shrinkage,
        content_vectors.reshape(tokens, 128),
        result_valve_scores.reshape(tokens, 128),
        jnp.swapaxes(stored_opening_memory[0], 1, 2).reshape(128, head_k),
        result_mapping_matrix.reshape(width, 128),
    )
    shape = jax.ShapeDtypeStruct
    outs = (
        shape((own_rows, width), BF16),
        shape((width, 128), BF16),
        shape((width, 128), BF16),
        shape((128, width), BF16),
        shape((64, 128), F32),
        shape((tokens, 64), BF16),
        shape((tokens, 64), BF16),
        shape((tokens, 64), F32),
        shape((tokens, 128), BF16),
        shape((tokens, 128), BF16),
    )
    vmem = pltpu.VMEM
    scratch = [
        vmem((n_tp, own_rows, 256), BF16),
        vmem((n_tp, own_rows, 256), BF16),
        vmem((n_sp, 8, 128), F32),
        vmem((n_sp, PITCH, 256), BF16),
        vmem((n_sp, PITCH, 256), BF16),
        vmem((rows, 128), BF16),
        vmem((rows, 128), BF16),
        vmem((rows, width), BF16),
        vmem((rows, width), BF16),
        vmem((width, 256), BF16),
        vmem((n_tp, rows, 128), BF16),
        vmem((n_tp, rows, 128), BF16),
        vmem((n_sp, PITCH, 128), BF16),
        vmem((n_sp, PITCH, 128), BF16),
        vmem((n_tp, own_rows, 128), BF16),
        vmem((n_tp, own_rows, 128), BF16),
        vmem((own_rows, width), BF16),
        vmem((n_tp, own_rows, width), BF16),
        vmem((n_sp, 16, 128), BF16),
        vmem((n_sp, 16, 128), BF16),
        vmem((n_sp, 16, 128), BF16),
        vmem((n_sp, 16, 128), BF16),
        vmem((n_z, 64, 128), BF16),
        vmem((n_z, 64, 128), BF16),
        vmem((n_z, 64, 128), BF16),
        vmem((n_z, 64, 128), BF16),
        vmem((n_z, 64, 128), BF16),
        vmem((n_tp, BLOCK, 128), BF16),
        vmem((n_tp, BLOCK, 128), BF16),
        vmem((n_tp, BLOCK + 16, 128), BF16),
        vmem((n_tp, BLOCK + 16, 128), BF16),
        vmem((padded, tokens), BF16),
        vmem((tokens, 2 * head_k), F32),
        vmem((tokens, 2 * head_k), F32),
        vmem((2, 128, head_k), F32),
        vmem((tokens, 128), F32),
        vmem((2, 128, head_k), F32),
        vmem((tokens, width), BF16),
        vmem((rows, 256), BF16),
        vmem((rows, 128), BF16),
        pltpu.SemaphoreType.DMA((15,)),
        pltpu.SemaphoreType.DMA((15,)),
    ]
    in_vmem = pl.BlockSpec(memory_space=pltpu.VMEM)

    def body(*refs):
        kernel(n_sp, n_tp, cap, *refs)

    results = pl.pallas_call(
        body,
        out_shape=outs,
        in_specs=[in_vmem] * len(args),
        out_specs=[in_vmem] * len(outs),
        scratch_shapes=scratch,
        compiler_params=pltpu.CompilerParams(
            collective_id=0, has_side_effects=True, vmem_limit_bytes=50 * 1024 * 1024
        ),
        name="layer_backward",
    )(*args)
    stream, gate, up, down, proj, query, key, retain, value, gig = results
    return (
        stream,
        gate[None],
        up[None],
        down[None],
        proj.reshape(64, 2, 64),
        query,
        key,
        retain,
        value.reshape(tokens, 2, 64),
        gig.reshape(tokens, 2, 64),
    )


def solution(mesh):
    both = ("sp", "tp")
    in_specs = (
        P(both, None),
        P(),
        P(both, None),
        P("sp", None),
        P("sp", None),
        P("sp", None, "tp"),
        P("sp", None, "tp"),
        P("sp", "tp", None),
        P("sp", None),
        P("sp", None),
        P("sp", None),
        P("sp", None),
        P("sp", None, "tp"),
        P("sp", None, "tp"),
        P("sp", None, None, "tp"),
        P(None, None, "tp"),
    )
    out_specs = (
        P(both, None),
        P("sp", None, "tp"),
        P("sp", None, "tp"),
        P("sp", "tp", None),
        P("sp", None, "tp"),
        P("sp", "tp"),
        P("sp", "tp"),
        P("sp", "tp"),
        P("sp", None, "tp"),
        P("sp", None, "tp"),
    )
    return jax.shard_map(
        on_device, mesh=mesh, in_specs=in_specs, out_specs=out_specs, check_vma=False
    )
```

time: 406 us -> 159 us (0.39)
  Pallas kernels: 0 us -> 144 us
  blocking collectives: 112 us -> 0 us
  other arithmetic: 68.6 us -> 0 us
  starting transfers between devices: 68.5 us -> 0 us
  local copies, waits for them, and re-layouts: 82.1 us -> 13.9 us
  waiting for transfers between devices: 47.9 us -> 0 us
  matrix products: 22.7 us -> 0 us
    pallas_call x0 -> x1, Pallas kernels: none -> 144 us  [on_device(): pl.pallas_call(body, out_shape=outs, in_specs=[in_vmem] * len(args), out_...]
    all_to_all x2 -> x0, blocking collectives: 76.8 us -> none  [the longest x1 39.4 us: on_device(): lax.all_to_all(outgoing, SP, split_axis=0, concat_axis=0, tiled=True)]
    all_to_all x10 -> x0, starting transfers between devices: 68.5 us -> none  [the longest x3 16.6 us: sum_at_owner(): lax.all_to_all(cut_along(shard, dim, length), axis, 0, 0, tiled=True)]
    all_to_all x10 -> x0, waiting for transfers between devices: 47.9 us -> none  [the longest x3 24.5 us: sum_at_owner(): lax.all_to_all(cut_along(shard, dim, length), axis, 0, 0, tiled=True)]
    all_gather x1 -> x0, blocking collectives: 35.2 us -> none  [carried_in(): decays = lax.all_gather(decay.reshape(-1), SP)]
    unnamed x31 -> x0, other arithmetic: 29.1 us -> none
    dot_general x16 -> x0, matrix products: 22.7 us -> none  [the longest x1 2.36 us: expert_backward(): lax.dot_general(inputs, gate_pre, contract_first, preferred_element_type=...]
    convert_element_type x10 -> x0, other arithmetic: 12.7 us -> none  [the longest x1 2.45 us: on_device(): decayed = key_weight.astype(jnp.bfloat16)]
  transfers between devices with their start and end apart: 10 -> 0, of which waited for: 6 -> 0; matrix products, arithmetic and copies ran while one was open for 23% -> 0% of each run, Pallas kernels for 0% -> 0%
where the time goes in v2:
time: 159 us
  Pallas kernels  144 us (91%)
  local copies, waits for them, and re-layouts  13.9 us (9%)
    pallas_call x1, Pallas kernels, on_device(): pl.pallas_call(body, out_shape=outs, in_specs=[in_vmem] * len(args), out_...  144 us
    unnamed x31, local copies, waits for them, and re-layouts  7.81 us

profile of v2, /device:TPU:1, one launch (start us, length us, event | category | flops | bytes accessed | tf_op | source)
XLA Modules:
  0.0 158.5 jit_solution(16926427237016708857)
XLA Ops:
  0.7 0.9 copy.38.refs_12_
  1.6 0.9 copy.39.refs_13_
  2.5 0.0 copy-done.9
  2.5 0.1 copy.36.refs_4_
  2.6 0.0 copy-start.8
  2.6 0.1 copy.37.refs_11_
  2.7 0.0 copy-start.1
  2.7 0.0 copy-start.2
  2.8 2.1 %copy.40.refs_15_ = bf16[2048,128]{1,0:T(8,128)(2,1)} copy(bf16[2048,128]{0,1:T(8,128)(2,1)} %bitcast.27) | data formatting | bytes 1048576 | tf_op jit(solution)/shard_map/reshape | solution.py:578
  4.9 0.0 copy-start.4
  4.9 0.9 copy-done.4
  5.9 0.8 copy-done.5
  6.6 0.8 copy-done.6
  7.4 143.8 %layer_backward.1 = (bf16[8,2048]{1,0:T(8,128)(2,1)S(1)}, bf16[2048,128]{1,0:T(8,128)(2,1)S(1)}, bf16[2048,128]{1,0:T(8,128)(2,1)S(1)}, bf16[128,2048]{1,0:T(8,1...) custom-call(bf16[8,2048]{1,0:T(8,128)(2,1)S(1)} %copy-done.5, ...), custom_call_target="tpu_custom_call" | custom-call | tf_op jit(solution)/shard_map/layer_backward/pallas_call | solution.py:643
  151.2 0.7 copy.43
  151.9 0.7 copy.44
  152.6 0.7 copy.45
  153.3 0.7 copy.41
  154.1 0.7 copy.42
  154.8 0.7 reshape.49
  155.5 0.6 copy.50
  156.1 0.8 copy.51
  156.9 0.8 copy.52
  157.7 0.8 copy.53
  (14 shorter events, 0.0 us)
Async XLA Ops:
  0.6 4.2 %copy-start.7 = (f32[2048]{0:T(1024)S(1)}, f32[2048]{0:T(1024)}, u32[]{:S(2)}) copy-start(f32[2048]{0:T(1024)} %param.17) | copy-start | bytes 24580
  0.7 1.9 %copy-start.10 = (f32[128,2]{0,1:T(2,128)S(1)}, f32[128,2]{0,1:T(2,128)}, u32[]{:S(2)}) copy-start(f32[128,2]{0,1:T(2,128)} %param.27) | copy-start | bytes 3076
  0.7 1.8 %copy-start.9 = (f32[128,2]{0,1:T(2,128)S(1)}, f32[128,2]{0,1:T(2,128)}, u32[]{:S(2)}) copy-start(f32[128,2]{0,1:T(2,128)} %param.20) | copy-start | bytes 3076
  0.7 4.2 %copy-start.3 = (bf16[128,1024]{1,0:T(8,128)(2,1)S(1)}, bf16[128,1024]{1,0:T(8,128)(2,1)}, u32[]{:S(2)}) copy-start(bf16[128,1024]{1,0:T(8,128)(2,1)} %refs_10_.1) | copy-start | bytes 786436
  2.6 2.3 %copy-start.8 = (s32[128,2]{0,1:T(2,128)S(1)}, s32[128,2]{0,1:T(2,128)}, u32[]{:S(2)}) copy-start(s32[128,2]{0,1:T(2,128)} %param.19) | copy-start | bytes 3076
  2.7 2.2 %copy-start = (bf16[1,2048,128]{2,1,0:T(8,128)(2,1)S(1)}, bf16[1,2048,128]{2,1,0:T(8,128)(2,1)}, u32[]{:S(2)}) copy-start(bf16[1,2048,128]{2,1,0:T(8,128)(2,1)} %param.21) | copy-start | bytes 1572868
  2.7 2.2 %copy-start.1 = (bf16[128,1024]{1,0:T(8,128)(2,1)S(1)}, bf16[128,1024]{1,0:T(8,128)(2,1)}, u32[]{:S(2)}) copy-start(bf16[128,1024]{1,0:T(8,128)(2,1)} %refs_8_.1) | copy-start | bytes 786436
  2.7 2.2 %copy-start.2 = (bf16[128,1024]{1,0:T(8,128)(2,1)S(1)}, bf16[128,1024]{1,0:T(8,128)(2,1)}, u32[]{:S(2)}) copy-start(bf16[128,1024]{1,0:T(8,128)(2,1)} %refs_9_.1) | copy-start | bytes 786436
  4.9 1.0 copy-start.4
  5.9 0.8 copy-start.5
  6.6 0.8 copy-start.6
